TPU v7x, 32 devices: a whole 2x2x4 slice. The times are simulated.
32 devices in a mesh: dp: 4 (over y, x), kv: 4 (over z), tp: 2 (over core).
Axes of the slice: x: 2, y: 2, z: 4, core: 2. Of those that a mesh axis runs over, the one named last changes fastest.
Arguments:
- tokens: bfloat16 [1024, 2048], P(('dp', 'kv', 'tp')), may hold values from -6 to 6
- norm_gain: float32 [2048], replicated, may hold values from 0.1 to 1.9
- gate_proj: bfloat16 [2048, 4096], P(None, ('kv', 'tp')), may hold values from -0.125 to 0.125
- inner_proj: bfloat16 [2048, 4096], P(None, ('kv', 'tp')), may hold values from -0.125 to 0.125
- write_proj: bfloat16 [2048, 1024], P(None, ('kv', 'tp')), may hold values from -0.125 to 0.125
- read_proj: bfloat16 [2048, 1024], P(None, ('kv', 'tp')), may hold values from -0.125 to 0.125
- step_proj: bfloat16 [2048, 64], replicated, may hold values from -0.125 to 0.125
- step_bias: float32 [64], replicated, may hold values from -3 to 0
- decay_log: float32 [64], replicated, may hold values from -5 to 0.7
- skip_gain: float32 [64], replicated, may hold values from 0.25 to 4
- conv_inner: bfloat16 [4, 4096], replicated, may hold values from -3 to 3
- conv_write: bfloat16 [4, 1024], replicated, may hold values from -3 to 3
- conv_read: bfloat16 [4, 1024], replicated, may hold values from -3 to 3
- out_gain: float32 [4096], replicated, may hold values from 0.1 to 1.9
- out_proj: bfloat16 [4096, 2048], P(('kv', 'tp')), may hold values from -0.09375 to 0.09375
- saved_state: float32 [256, 64, 64, 128], P('dp', ('kv', 'tp')), may hold values from -1.75 to 1.75
- inner_history: bfloat16 [256, 7, 4096], P('dp', None, ('kv', 'tp')), may hold values from -6 to 6
- write_history: bfloat16 [256, 7, 1024], P('dp', None, ('kv', 'tp')), may hold values from -6 to 6
- read_history: bfloat16 [256, 7, 1024], P('dp', None, ('kv', 'tp')), may hold values from -6 to 6
- last_steps: float32 [256, 4, 64], P('dp', None, ('kv', 'tp')), may hold values from 0.02 to 1
- accepted: int32 [256], P('dp'), may hold values from 0 to 4
Outputs:
- mixed: bfloat16 [1024, 2048], P(('dp', 'kv', 'tp'))
- base_state: float32 [256, 64, 64, 128], P('dp', ('kv', 'tp'))
All inputs are finite; a program needn't handle non-finite values.
Results may differ from a plain program's by a relative error of at most 0.014.
Values may be sent and summed in bfloat16 or wider, within the bound.
A program may use at most 128 MiB of HBM per device.

v0:
```python
import jax
import jax.numpy as jnp
from jax import lax
from jax.sharding import PartitionSpec as P

GROUPS = 8
INNER = 4096


EPSILON = 0.1
highest = lax.Precision.HIGHEST


def shortened(shard):

    def short(part):
        return part.astype(jnp.bfloat16) if part.dtype == jnp.float32 else part

    return jax.tree.map(short, shard)


def swapped(value, axis, stride):
    mask = 2**stride
    pairs = [(source, source ^ mask) for source in range(lax.axis_size(axis))]
    return lax.ppermute(value, axis, pairs)


def conv_rows(row_block, weight):
    out_len = row_block.shape[1] - weight.shape[0] + 1
    result = weight[0] * row_block[:, 0:out_len]
    for offset in range(1, weight.shape[0]):
        result = result + weight[offset] * row_block[:, offset : offset + out_len]
    return result


def body(
    tokens,
    norm_gain,
    gate_proj,
    inner_proj,
    write_proj,
    read_proj,
    step_proj,
    step_bias,
    decay_log,
    skip_gain,
    conv_inner,
    conv_write,
    conv_read,
    out_gain,
    out_proj,
    saved_state,
    inner_history,
    write_history,
    read_history,
    last_steps,
    accepted,
):
    device_rank = lax.axis_index(("kv", "tp"))
    seq_count = saved_state.shape[0]
    local_heads = saved_state.shape[1]
    head_dim = saved_state.shape[2]
    proposals = last_steps.shape[1]
    inner_cols = inner_proj.shape[1]
    state_cols = write_proj.shape[1]
    token_count = tokens.shape[0]
    own_rows = tokens.astype(jnp.float32)
    normed_own = (
        own_rows
        * lax.rsqrt(jnp.mean(own_rows * own_rows, axis=-1, keepdims=True) + EPSILON)
        * norm_gain
    ).astype(jnp.bfloat16)
    normed = lax.all_gather(normed_own, ("kv", "tp"), axis=0, tiled=True)
    gate_rows = jnp.dot(normed, gate_proj, preferred_element_type=jnp.float32).astype(jnp.bfloat16)
    inner_rows = jnp.dot(normed, inner_proj, preferred_element_type=jnp.float32).astype(
        jnp.bfloat16
    )
    write_rows = jnp.dot(normed, write_proj, preferred_element_type=jnp.float32).astype(
        jnp.bfloat16
    )
    read_rows = jnp.dot(normed, read_proj, preferred_element_type=jnp.float32).astype(jnp.bfloat16)
    first_head = device_rank * local_heads
    step_weight = lax.dynamic_slice_in_dim(step_proj, first_head, local_heads, 1)
    step_rows = jnp.dot(normed, step_weight, preferred_element_type=jnp.float32)
    taps_inner = lax.dynamic_slice_in_dim(
        conv_inner, device_rank * inner_cols, inner_cols, 1
    ).astype(jnp.float32)
    taps_write = lax.dynamic_slice_in_dim(
        conv_write, device_rank * state_cols, state_cols, 1
    ).astype(jnp.float32)
    taps_read = lax.dynamic_slice_in_dim(conv_read, device_rank * state_cols, state_cols, 1).astype(
        jnp.float32
    )
    conv_width = conv_inner.shape[0]
    window_rows = accepted[:, None] + jnp.arange(conv_width - 1, dtype=jnp.int32)[None, :]

    def current(history, new_rows, weight):
        window = jnp.take_along_axis(history, window_rows[:, :, None], axis=1)
        joined = jnp.concatenate([window, new_rows.reshape(seq_count, proposals, -1)], axis=1)
        return jax.nn.silu(conv_rows(joined.astype(jnp.float32), weight))

    inner_old = jax.nn.silu(conv_rows(inner_history.astype(jnp.float32), taps_inner))
    write_old = jax.nn.silu(conv_rows(write_history.astype(jnp.float32), taps_write)).astype(
        jnp.bfloat16
    )
    inner_new = current(inner_history, inner_rows, taps_inner)
    write_new = current(write_history, write_rows, taps_write).astype(jnp.bfloat16)
    read_new = current(read_history, read_rows, taps_read).astype(jnp.bfloat16)
    write_both = jnp.concatenate([write_old, write_new], axis=1)
    group_span = lax.axis_size("kv") * lax.axis_size("tp") // GROUPS
    pieces = (write_both, read_new)
    if group_span >= 2:
        pieces = (
            lax.all_gather(pieces[0], "tp", axis=2, tiled=True),
            lax.all_gather(pieces[1], "tp", axis=2, tiled=True),
        )
        kv_rank = lax.axis_index("kv")
        bit_count = (group_span // lax.axis_size("tp")).bit_length() - 1
        for bit in range(bit_count):
            partner = swapped((shortened(pieces[0]), shortened(pieces[1])), "kv", bit)
            lower = jnp.bitwise_and(jnp.right_shift(kv_rank, bit), 1) == 0
            pieces = tuple(
                (
                    jnp.where(
                        lower,
                        jnp.concatenate([mine, theirs], axis=2),
                        jnp.concatenate([theirs, mine], axis=2),
                    )
                    for mine, theirs in zip(pieces, partner)
                )
            )
    write_group = pieces[0].astype(jnp.float32)
    read_group = pieces[1].astype(jnp.float32)
    write_past = write_group[:, :proposals]
    write_next = write_group[:, proposals:]
    decay_rate = -jnp.exp(lax.dynamic_slice_in_dim(decay_log, first_head, local_heads, 0))
    skip_local = lax.dynamic_slice_in_dim(skip_gain, first_head, local_heads, 0)
    bias_local = lax.dynamic_slice_in_dim(step_bias, first_head, local_heads, 0)
    step_size = jax.nn.softplus(step_rows + bias_local[None, :]).reshape(
        seq_count, proposals, local_heads
    )
    accepted_mask = (jnp.arange(proposals, dtype=jnp.int32)[None, :] < accepted[:, None]).astype(
        jnp.float32
    )
    step_logs = decay_rate[None, None, :] * last_steps * accepted_mask[:, :, None]
    total_log = jnp.sum(step_logs, axis=1)
    tail_log = total_log[:, None, :] - jnp.cumsum(step_logs, axis=1)
    old_weights = accepted_mask[:, :, None] * jnp.exp(tail_log) * last_steps
    inner_old_heads = inner_old.reshape(seq_count, proposals, local_heads, head_dim)
    base_state = jnp.exp(total_log)[:, :, None, None] * saved_state + jnp.einsum(
        "sth,sthp,stn->shpn", old_weights, inner_old_heads, write_past, precision=highest
    )
    cumulative = jnp.cumsum(decay_rate[None, None, :] * step_size, axis=1)
    log_gap = cumulative[:, :, None, :] - cumulative[:, None, :, :]
    causal = (jnp.arange(proposals)[:, None] >= jnp.arange(proposals)[None, :])[None, :, :, None]
    kernel = jnp.where(causal, jnp.exp(jnp.where(causal, log_gap, 0.0)), 0.0)
    scores = jnp.einsum("sin,sjn->sij", read_group, write_next, precision=highest)
    inner_heads = inner_new.reshape(seq_count, proposals, local_heads, head_dim)
    within = jnp.einsum(
        "sijh,sjh,sjhp->sihp", kernel * scores[..., None], step_size, inner_heads, precision=highest
    )
    carried = jnp.exp(cumulative)[..., None] * jnp.einsum(
        "sin,shpn->sihp", read_group, base_state, precision=highest
    )
    mixed_heads = within + carried + skip_local[None, None, :, None] * inner_heads
    gated_rows = mixed_heads.reshape(seq_count * proposals, inner_cols) * jax.nn.silu(
        gate_rows.astype(jnp.float32)
    )
    gain_local = lax.dynamic_slice_in_dim(out_gain, device_rank * inner_cols, inner_cols, 0)
    squares = jnp.sum(gated_rows * gated_rows, axis=-1)
    unscaled = (gated_rows * gain_local).astype(jnp.bfloat16)
    partial_value = jnp.dot(unscaled, out_proj, preferred_element_type=jnp.float32)
    square_total = lax.psum(squares, ("kv", "tp"))
    summed = lax.psum_scatter(partial_value, ("kv", "tp"), scatter_dimension=0, tiled=True)
    square_own = lax.dynamic_slice_in_dim(square_total, device_rank * token_count, token_count, 0)
    mixed = (summed * lax.rsqrt(square_own / INNER + EPSILON)[:, None]).astype(jnp.bfloat16)
    return (mixed, base_state)


def solution(mesh):
    placed = (
        P(("dp", "kv", "tp"), None),
        P(),
        P(None, ("kv", "tp")),
        P(None, ("kv", "tp")),
        P(None, ("kv", "tp")),
        P(None, ("kv", "tp")),
        P(),
        P(),
        P(),
        P(),
        P(),
        P(),
        P(),
        P(),
        P(("kv", "tp"), None),
        P("dp", ("kv", "tp"), None, None),
        P("dp", None, ("kv", "tp")),
        P("dp", None, ("kv", "tp")),
        P("dp", None, ("kv", "tp")),
        P("dp", None, ("kv", "tp")),
        P("dp"),
    )
    return jax.shard_map(
        body,
        mesh=mesh,
        in_specs=placed,
        out_specs=(P(("dp", "kv", "tp"), None), P("dp", ("kv", "tp"), None, None)),
        check_vma=False,
    )
```

profile of v0, /device:TPU:0, one launch (start us, length us, event | category | flops | bytes accessed | tf_op | source)
XLA Modules:
  0.0 169.7 jit_solution(11714360509168293512)
XLA Ops:
  7.2 1.2 fusion.21
  8.5 1.7 fusion.23
  13.0 1.6 convert_element_type.84
  14.6 3.3 %gather_fusion.2 = bf16[192,128]{1,0:T(8,128)(2,1)S(1)} fusion(bf16[64,7,128]{2,0,1:T(8,128)(2,1)} %param.40, s32[192]{0:T(256)S(1)} %reshape.196), kind=kCustom, calls=%fused_computation.1.clone | custom fusion | bytes 99840 | tf_op jit(solution)/shard_map/jit(take_along_axis)/gather | solution.py:98
  17.9 3.4 %gather_fusion = bf16[192,512]{1,0:T(8,128)(2,1)} fusion(bf16[64,7,512]{2,0,1:T(8,128)(2,1)S(1)} %copy-done.1, s32[192]{0:T(256)S(1)} %reshape.196), kind=kCustom, calls=%fused_computation.2 | custom fusion | bytes 394752 | tf_op jit(solution)/shard_map/jit(take_along_axis)/gather | solution.py:98
  21.5 3.3 %gather_fusion.1 = bf16[192,128]{1,0:T(8,128)(2,1)S(1)} fusion(bf16[64,7,128]{2,0,1:T(8,128)(2,1)} %param.41, s32[192]{0:T(256)S(1)} %reshape.196), kind=kCustom, calls=%fused_computation.clone | custom fusion | bytes 99840 | tf_op jit(solution)/shard_map/jit(take_along_axis)/gather | solution.py:98
  34.9 1.2 dynamic_slice.33
  36.2 1.3 dynamic_slice.34
  40.1 1.9 %convolution_convert_fusion.3 = bf16[256,128]{1,0:T(8,128)(2,1)S(1)} fusion(bf16[256,2048]{1,0:T(8,128)(2,1)} %all-gather.2.cloned.1.call-done, bf16[2048,128]{1,0:T(8,128)(2,1)} %param.28), kind=kOutput, calls=%fused_computation.12 | convolution fusion | flops 134250496 | bytes 1638400 | tf_op jit(solution)/shard_map/dot_general | solution.py:81
  47.4 1.8 %convolution_convert_fusion.2 = bf16[256,128]{1,0:T(8,128)(2,1)S(1)} fusion(bf16[256,2048]{1,0:T(8,128)(2,1)} %all-gather.2.cloned.1.call-done, bf16[2048,128]{1,0:T(8,128)(2,1)} %param.27), kind=kOutput, calls=%fused_computation.11 | convolution fusion | flops 134250496 | bytes 1638400 | tf_op jit(solution)/shard_map/dot_general | solution.py:78
  49.9 3.3 %convolution_convert_fusion.1 = bf16[256,512]{1,0:T(8,128)(2,1)} fusion(bf16[256,2048]{1,0:T(8,128)(2,1)} %all-gather.2.cloned.1.call-done, bf16[2048,512]{1,0:T(8,128)(2,1)} %param.26), kind=kOutput, calls=%fused_computation.9 | convolution fusion | flops 537001984 | bytes 3407872 | tf_op jit(solution)/shard_map/dot_general | solution.py:75
  54.3 1.4 divide_multiply_fusion.1
  55.7 1.3 reshape.182
  57.0 2.1 %copy.101 = f32[64,4,8]{1,2,0:T(8,128)} copy(f32[64,4,8]{2,1,0:T(4,128)} %exp.54) | data formatting | bytes 16384 | tf_op jit(solution)/shard_map/exp | solution.py:162
  59.1 2.2 %reshape.179 = f32[64,4,8,64]{3,2,0,1:T(8,128)} reshape(f32[64,4,512]{2,0,1:T(8,128)} %get-tuple-element.7) | data formatting | bytes 1048576 | tf_op jit(solution)/shard_map/reshape | solution.py:158
  64.8 21.0 %multiply_add_fusion = f32[64,8,64,128]{3,2,1,0:T(8,128)} fusion(f32[64,8,64,128]{3,2,1,0:T(8,128)} %param.38, f32[64,8]{1,0:T(8,128)S(1)} %copy-done.12, f32[64,4,8,64]{3,2,0,1:T(8,128)S(1)} %reshape.182, f32[64,4,8]{1,2,0:T(8,128)S(1)} %copy-done.6, bf16[64,4,128,1]{2,0,1,3:T(8,128)(2,1)S(1)} %get-tuple-element.14), kind=kOutput, calls=%fused_computation.3 | convolution fusion | flops 209846272 | bytes 34154496 | tf_op jit(solution)/shard_map/sth,sthp,stn->shpn/dot_general | solution.py:150
  85.8 23.1 %convolution_multiply_fusion = f32[64,4,8,64]{3,1,2,0:T(4,128)S(1)} fusion(f32[64,8,64,128]{3,2,1,0:T(8,128)} %multiply_add_fusion, f32[64,4,8]{1,2,0:T(8,128)S(1)} %copy-done.7, bf16[64,4,128,1]{2,0,1,3:T(8,128)(2,1)S(1)} %copy-done.9), kind=kOutput, calls=%fused_computation.7 | convolution fusion | flops 201457664 | bytes 17375232 | tf_op jit(solution)/shard_map/sin,shpn->sihp/dot_general | solution.py:162
  108.9 5.1 %fusion.1 = f32[64,4,8,64]{3,1,2,0:T(4,128)S(1)} fusion(f32[64,4,8,64]{3,1,2,0:T(4,128)S(1)} %convolution_multiply_fusion, f32[64,4,8,64]{3,2,0,1:T(8,128)S(1)} %copy-done.4, f32[64,4,8,64]{3,2,0,1:T(8,128)S(1)} %broadcast_multiply_fusion, f32[8]{0:T(128)S(1)} %copy-done.18, f32[64,4,4]{2,1,0:T(4,128)S(1)} %fusion.37, f32[64,4,8]{1,2,0:T(8,128)S(1)} %copy-done.10, ...), kind=kOutput, calls=%fused_computation.6 | convolution fusion | flops 6717440 | bytes 2109488 | tf_op jit(solution)/shard_map/sijh,sjh,sjhp->sihp/dot_general | solution.py:159
  115.1 2.3 %reshape.183 = f32[256,512]{1,0:T(8,128)} reshape(f32[64,4,8,64]{3,2,1,0:T(8,128)} %copy.113) | data formatting | bytes 1048576 | tf_op jit(solution)/shard_map/reshape | solution.py:166
  117.4 2.5 %multiply_reduce_fusion = (f32[256]{0:T(256)S(1)}, f32[256,512]{1,0:T(8,128)S(1)}) fusion(f32[256,512]{1,0:T(8,128)} %reshape.183, bf16[256,2048]{1,0:T(8,128)(2,1)S(1)} %copy-done.3, bf16[2048,512]{1,0:T(8,128)(2,1)} %param.25), kind=kOutput, calls=%fused_computation.36 | convolution fusion | flops 538050304 | bytes 4195328 | tf_op jit(solution)/shard_map/dot_general | solution.py:74
  120.0 2.1 %fusion.24 = f32[256,2048]{1,0:T(8,128)} fusion(bf16[512,2048]{1,0:T(8,128)(2,1)S(1)} %copy-done, f32[256,512]{1,0:T(8,128)S(1)} %get-tuple-element.24, f32[512]{0:T(512)S(1)} %copy-done.14), kind=kOutput, calls=%fused_computation.54 | convolution fusion | flops 537133056 | bytes 4720640 | tf_op jit(solution)/shard_map/dot_general | solution.py:172
  122.1 18.3 %psum.7 = f32[256]{0:T(256)S(1)} all-reduce(f32[256]{0:T(256)S(1)} %get-tuple-element.23), channel_id=1, replica_groups=mesh['dp'=4,'kv'=4,'tp'=2] {'kv','tp'}, use_global_device_ids=true, to_apply=%region_6.8 | all-reduce | flops 256 | bytes 2048 | tf_op jit(solution)/shard_map/psum | solution.py:173
  140.5 20.7 %reduce-scatter.2.cloned.1.call-done = f32[32,2048]{1,0:T(8,128)} async-done(((f32[256,2048]{1,0:T(8,128)}), f32[32,2048]{1,0:T(8,128)}) %reduce-scatter.2.cloned.1.call-update) | async-done | bytes 262160 | tf_op jit(solution)/shard_map/reduce_scatter | solution.py:174
  161.2 1.7 multiply_convert_fusion.2
  (101 shorter events, 27.4 us)
Async XLA Ops:
  7.2 112.8 %copy-start = (bf16[512,2048]{1,0:T(8,128)(2,1)S(1)}, bf16[512,2048]{1,0:T(8,128)(2,1)}, u32[]{:S(2)}) copy-start(bf16[512,2048]{1,0:T(8,128)(2,1)} %param.37) | copy-start | bytes 6291460
  7.2 10.7 %copy-start.1 = (bf16[64,7,512]{2,0,1:T(8,128)(2,1)S(1)}, bf16[64,7,512]{2,0,1:T(8,128)(2,1)}, u32[]{:S(2)}) copy-start(bf16[64,7,512]{2,0,1:T(8,128)(2,1)} %param.39) | copy-start | bytes 1376260
  7.2 32.9 %all-gather.2.cloned.1.call-start = ((), (), s32[]{:S(2)}) async-start(), calls=%async_computation.1 | async-start | bytes 1179648 | tf_op jit(solution)/shard_map/all_gather | solution.py:73
  10.2 151.0 %reduce-scatter.2.cloned.1.call-start = ((), (), s32[]{:S(2)}) async-start(), calls=%async_computation.2 | async-start | bytes 2359296 | tf_op jit(solution)/shard_map/reduce_scatter | solution.py:174
  21.4 7.7 %copy-start.13 = (f32[64,4,8]{0,2,1:T(8,128)S(1)}, f32[64,4,8]{0,2,1:T(8,128)}, u32[]{:S(2)}) copy-start(f32[64,4,8]{0,2,1:T(8,128)} %param.42) | copy-start | bytes 24580
  21.4 8.4 %copy-start.15 = (s32[64]{0:T(128)S(1)}, s32[64]{0:T(128)}, u32[]{:S(2)}) copy-start(s32[64]{0:T(128)} %param.43) | copy-start | bytes 772
  29.0 0.6 copy-start.16
  40.0 4.7 %copy-start.17 = (f32[8]{0:T(128)S(1)}, f32[8]{0:T(128)}, u32[]{:S(2)}) copy-start(f32[8]{0:T(128)} %copy-done.16) | copy-start | bytes 100
  40.1 3.3 %copy-start.2 = (bf16[256,2048]{1,0:T(8,128)(2,1)S(1)}, bf16[256,2048]{1,0:T(8,128)(2,1)}, u32[]{:S(2)}) copy-start(bf16[256,2048]{1,0:T(8,128)(2,1)} %all-gather.2.cloned.1.call-done) | copy-start | bytes 3145732
  55.7 5.6 %copy-start.11 = (bf16[64,3,128]{2,0,1:T(8,128)(2,1)S(1)}, bf16[64,3,128]{2,0,1:T(8,128)(2,1)}, u32[]{:S(2)}) copy-start(bf16[64,3,128]{2,0,1:T(8,128)(2,1)} %copy.96) | copy-start | bytes 147460
  55.7 6.6 %copy-start.5 = (f32[64,7,128]{2,0,1:T(8,128)S(1)}, f32[64,7,128]{2,0,1:T(8,128)}, u32[]{:S(2)}) copy-start(f32[64,7,128]{2,0,1:T(8,128)} %convert_element_type.84) | copy-start | bytes 688132
  57.0 7.2 %copy-start.8 = (f32[64,4,8]{2,0,1:T(8,128)S(1)}, f32[64,4,8]{2,0,1:T(8,128)}, u32[]{:S(2)}) copy-start(f32[64,4,8]{2,0,1:T(8,128)} %copy.88) | copy-start | bytes 24580
  61.4 2.8 %copy-start.4 = (f32[64,4,8,64]{3,2,0,1:T(8,128)S(1)}, f32[64,4,8,64]{3,2,0,1:T(8,128)}, u32[]{:S(2)}) copy-start(f32[64,4,8,64]{3,2,0,1:T(8,128)} %reshape.179) | copy-start | bytes 1572868
  61.4 3.4 %copy-start.6 = (f32[64,4,8]{1,2,0:T(8,128)S(1)}, f32[64,4,8]{1,2,0:T(8,128)}, u32[]{:S(2)}) copy-start(f32[64,4,8]{1,2,0:T(8,128)} %copy.108) | copy-start | bytes 24580
  61.4 3.4 %copy-start.12 = (f32[64,8]{1,0:T(8,128)S(1)}, f32[64,8]{1,0:T(8,128)}, u32[]{:S(2)}) copy-start(f32[64,8]{1,0:T(8,128)} %copy.105) | copy-start | bytes 6148
  64.8 21.0 %copy-start.7 = (f32[64,4,8]{1,2,0:T(8,128)S(1)}, f32[64,4,8]{1,2,0:T(8,128)}, u32[]{:S(2)}) copy-start(f32[64,4,8]{1,2,0:T(8,128)} %copy.101) | copy-start | bytes 24580
  64.8 21.0 %copy-start.9 = (bf16[64,4,128,1]{2,0,1,3:T(8,128)(2,1)S(1)}, bf16[64,4,128,1]{2,0,1,3:T(8,128)(2,1)}, u32[]{:S(2)}) copy-start(bf16[64,4,128,1]{2,0,1,3:T(8,128)(2,1)} %fusion.67) | copy-start | bytes 196612
  85.8 23.1 %copy-start.10 = (f32[64,4,8]{1,2,0:T(8,128)S(1)}, f32[64,4,8]{1,2,0:T(8,128)}, u32[]{:S(2)}) copy-start(f32[64,4,8]{1,2,0:T(8,128)} %copy.92) | copy-start | bytes 24580
  85.8 23.1 %copy-start.18 = (f32[8]{0:T(128)S(1)}, f32[8]{0:T(128)}, u32[]{:S(2)}) copy-start(f32[8]{0:T(128)} %dynamic_slice.33) | copy-start | bytes 100
  85.8 23.1 %copy-start.19 = (pred[4,4]{1,0:T(4,128)(4,1)S(1)}, pred[4,4]{1,0:T(4,128)(4,1)}, u32[]{:S(2)}) copy-start(pred[4,4]{1,0:T(4,128)(4,1)} %iota_compare_fusion.1) | copy-start | bytes 52
  114.1 3.4 %copy-start.3 = (bf16[256,2048]{1,0:T(8,128)(2,1)S(1)}, bf16[256,2048]{1,0:T(8,128)(2,1)}, u32[]{:S(2)}) copy-start(bf16[256,2048]{1,0:T(8,128)(2,1)} %all-gather.2.cloned.1.call-done) | copy-start | bytes 3145732
  117.4 2.6 %copy-start.14 = (f32[512]{0:T(512)S(1)}, f32[512]{0:T(512)}, u32[]{:S(2)}) copy-start(f32[512]{0:T(512)} %dynamic_slice.34) | copy-start | bytes 6148
Sparse Core Ops, SparseCore 0:
  10.3 24.9 all-gather.1
  122.2 38.9 reduce-scatter.1
where the time goes:
time: 171 us; the launch traced here: 170 us
  matrix products  63 us (37%)
  local copies, waits for them, and re-layouts  34.5 us (20%)
  waiting for transfers between devices  20.8 us (12%)
  other arithmetic  18.6 us (11%)
  blocking collectives  18.3 us (11%)
  between operations  14.5 us (8%)
    dot_general x1, matrix products, body(): jnp.einsum('sin,shpn->sihp', read_group, base_state, precision=highest)  23.1 us
    dot_general x1, matrix products, body(): jnp.einsum('sth,sthp,stn->shpn', old_weights, inner_old_heads, write_past...  21 us
    reduce_scatter x1, waiting for transfers between devices, body(): lax.psum_scatter(partial_value, ('kv', 'tp'), scatter_dimension=0, tiled=...  20.7 us
    psum x1, blocking collectives, body(): square_total = lax.psum(squares, ('kv', 'tp'))  18.3 us
    gather x7, local copies, waits for them, and re-layouts, current(): window = jnp.take_along_axis(history, window_rows[:, :, None], axis=1)  11.3 us
    dot_general x1, matrix products, body(): jnp.einsum('sijh,sjh,sjhp->sihp', kernel * scores[..., None], step_size,...  5.11 us
  transfers between devices with their start and end apart: 2, of which 1 were waited for; matrix products, arithmetic and copies ran while one was open for 17% of the time, Pallas kernels for 0%

commit v1 on v0

v1 whole, which is shorter than its diff:
```python
import functools

import jax
import jax.numpy as jnp
from jax import lax
from jax.experimental import pallas as pl
from jax.experimental.pallas import tpu as pltpu
from jax.sharding import PartitionSpec as P

GROUPS = 8
EPSILON = 0.1
BLOCK = 8
highest = lax.Precision.HIGHEST


def swapped(value, axis, stride):
    mask = 2**stride
    pairs = [(source, source ^ mask) for source in range(lax.axis_size(axis))]
    return lax.ppermute(value, axis, pairs)


def mix_kernel(
    rank_ref,
    acc_ref,
    steps_ref,
    last_ref,
    par_ref,
    gate_ref,
    inner_ref,
    write_ref,
    read_ref,
    hist_inner_ref,
    hist_write_ref,
    hist_read_ref,
    taps_inner_ref,
    taps_write_ref,
    taps_read_ref,
    gain_ref,
    expand_ref,
    state_ref,
    un_ref,
    sq_ref,
    base_ref,
):
    f32 = jnp.float32
    props = steps_ref.shape[0]
    heads = steps_ref.shape[2]
    cols = inner_ref.shape[2]
    states = write_ref.shape[2]
    head_dim = cols // heads
    hist = hist_inner_ref.shape[0]
    width = taps_inner_ref.shape[0]
    acc = acc_ref[...]

    def silu(x):
        return x / (1.0 + jnp.exp(-x))

    def slabs(ref):
        return [ref[k].astype(f32) for k in range(ref.shape[0])]

    def conv(rows, taps_ref):
        taps = taps_ref[...].astype(f32)
        res = []
        for r in range(len(rows) - width + 1):
            v = taps[0:1] * rows[r]
            for k in range(1, width):
                v = v + taps[k : k + 1] * rows[r + k]
            res.append(silu(v))
        return res

    def current(h, new_ref):
        where_at = jnp.broadcast_to(acc, h[0].shape)
        rows = []
        for k in range(width - 1):
            r = h[k]
            for v in range(1, hist - width + 2):
                r = jnp.where(where_at == v, h[k + v], r)
            rows.append(r)
        return rows + slabs(new_ref)

    h_inner = slabs(hist_inner_ref)
    inner_old = conv(h_inner, taps_inner_ref)
    inner_new = conv(current(h_inner, inner_ref), taps_inner_ref)
    h_write = slabs(hist_write_ref)
    round_bf = lambda x: x.astype(jnp.bfloat16).astype(f32)
    write_old = [round_bf(x) for x in conv(h_write, taps_write_ref)]
    write_new = [round_bf(x) for x in conv(current(h_write, write_ref), taps_write_ref)]
    read_new = [round_bf(x) for x in conv(current(slabs(hist_read_ref), read_ref), taps_read_ref)]

    bias = par_ref[0:1]
    rate = -jnp.exp(par_ref[1:2])
    skip = par_ref[2:3]
    acc_h = jnp.broadcast_to(acc, (BLOCK, heads))
    masks = [jnp.where(acc_h > t, 1.0, 0.0) for t in range(props)]
    logs = [rate * last_ref[t] * masks[t] for t in range(props)]
    coefs = [None] * props
    tail = jnp.zeros((BLOCK, heads), f32)
    for t in reversed(range(props)):
        coefs[t] = masks[t] * jnp.exp(tail) * last_ref[t]
        tail = tail + logs[t]
    decay = jnp.exp(tail)
    step = []
    for t in range(props):
        x = steps_ref[t] + bias
        step.append(jnp.maximum(x, 0.0) + jnp.log1p(jnp.exp(-jnp.abs(x))))
    cums = []
    for t in range(props):
        cums.append(rate * step[t] + (cums[-1] if cums else 0.0))
    where_of = {}
    for i in range(props):
        for j in range(i + 1):
            score = jnp.sum(read_new[i] * write_new[j], axis=-1, keepdims=True)
            c = jnp.exp(cums[i] - cums[j]) * step[j] * score
            if i == j:
                c = c + skip
            where_of[(i, j)] = len(coefs)
            coefs.append(c)
    first_cum = len(coefs)
    for i in range(props):
        coefs.append(jnp.exp(cums[i]))
    wide = jnp.dot(
        jnp.concatenate(coefs, axis=0),
        expand_ref[...],
        precision=highest,
        preferred_element_type=f32,
    )

    def at(k):
        return wide[k * BLOCK : (k + 1) * BLOCK]

    left = jnp.concatenate([at(t) * inner_old[t] for t in range(props)], axis=0)
    high = round_bf(left)
    both = jnp.concatenate([high, left - high], axis=0)
    turned = jnp.transpose(both).astype(jnp.bfloat16)
    write_all = jnp.concatenate(write_old + write_old, axis=0)
    read_all = jnp.concatenate(read_new, axis=0)
    seq_w = lax.broadcasted_iota(jnp.int32, write_all.shape, 0) % BLOCK
    seq_r = lax.broadcasted_iota(jnp.int32, read_all.shape, 0) % BLOCK
    carried = jnp.zeros((props * BLOCK, cols), f32)
    for s in range(BLOCK):
        right = jnp.where(seq_w == s, write_all, 0.0).astype(jnp.bfloat16)
        update = jnp.dot(turned, right, preferred_element_type=f32)
        parts = []
        for h in range(heads):
            lo, hi = h * head_dim, (h + 1) * head_dim
            d = jnp.broadcast_to(decay[s : s + 1, h : h + 1], (head_dim, states))
            new = d * state_ref[s, lo:hi, :] + update[lo:hi]
            base_ref[s, lo:hi, :] = new
            parts.append(new.astype(jnp.bfloat16))
        asked = jnp.where(seq_r == s, read_all, 0.0).astype(jnp.bfloat16)
        carried = carried + lax.dot_general(
            asked,
            jnp.concatenate(parts, axis=0),
            (((1,), (1,)), ((), ())),
            preferred_element_type=f32,
        )
    for i in range(props):
        y = at(first_cum + i) * carried[i * BLOCK : (i + 1) * BLOCK]
        for j in range(i + 1):
            y = y + at(where_of[(i, j)]) * inner_new[j]
        g = y * silu(gate_ref[i].astype(f32))
        sq_ref[i] = jnp.broadcast_to(jnp.sum(g * g, axis=-1, keepdims=True), sq_ref.shape[1:])
        un_ref[i] = (g * gain_ref[...]).astype(un_ref.dtype)


def mix(rank, group, acc, steps, last, par, gate, inner, write, read, hi, hw, hr, ci, cw, cr, gain, state):
    props, seqs, heads = steps.shape
    cols, states = state.shape[1], state.shape[2]
    expand = (jnp.arange(cols)[None, :] // (cols // heads) == jnp.arange(heads)[:, None]).astype(
        jnp.float32
    )
    hist = hi.shape[0]
    width = ci.shape[0]

    def slab(lead, last_dim):
        return pl.BlockSpec((lead, BLOCK, last_dim), lambda g, r: (0, g, 0))

    def own(rows, last_dim, which):
        return pl.BlockSpec((rows, last_dim), lambda g, r: (0, r[which]))

    state_spec = pl.BlockSpec((BLOCK, cols, states), lambda g, r: (g, 0, 0))
    return pl.pallas_call(
        mix_kernel,
        grid_spec=pltpu.PrefetchScalarGridSpec(
            num_scalar_prefetch=1,
            grid=(seqs // BLOCK,),
            in_specs=[
                pl.BlockSpec((BLOCK, 1), lambda g, r: (g, 0)),
                slab(props, heads),
                slab(props, heads),
                pl.BlockSpec(par.shape, lambda g, r: (0, 0)),
                slab(props, cols),
                slab(props, cols),
                slab(props, states),
                slab(props, states),
                slab(hist, cols),
                slab(hist, states),
                slab(hist, states),
                own(width, cols, 0),
                own(width, states, 1),
                own(width, states, 1),
                own(1, cols, 0),
                pl.BlockSpec(expand.shape, lambda g, r: (0, 0)),
                state_spec,
            ],
            out_specs=[slab(props, cols), slab(props, 128), state_spec],
        ),
        out_shape=[
            jax.ShapeDtypeStruct((props, seqs, cols), jnp.bfloat16),
            jax.ShapeDtypeStruct((props, seqs, 128), jnp.float32),
            jax.ShapeDtypeStruct(state.shape, jnp.float32),
        ],
        compiler_params=pltpu.CompilerParams(
            dimension_semantics=("arbitrary",), vmem_limit_bytes=48 * 1024 * 1024
        ),
        name="mix",
    )(
        jnp.stack([rank, group]).astype(jnp.int32),
        acc, steps, last, par, gate, inner, write, read, hi, hw, hr, ci, cw, cr, gain, expand, state,
    )


def gathered(own):
    return lax.all_gather(own, ("kv", "tp"), axis=0, tiled=True)


def body(
    tokens,
    norm_gain,
    gate_proj,
    inner_proj,
    write_proj,
    read_proj,
    step_proj,
    step_bias,
    decay_log,
    skip_gain,
    conv_inner,
    conv_write,
    conv_read,
    out_gain,
    out_proj,
    saved_state,
    inner_history,
    write_history,
    read_history,
    last_steps,
    accepted,
):
    device_rank = lax.axis_index(("kv", "tp"))
    seq_count = saved_state.shape[0]
    local_heads = saved_state.shape[1]
    head_dim = saved_state.shape[2]
    proposals = last_steps.shape[1]
    inner_cols = inner_proj.shape[1]
    state_cols = write_proj.shape[1]
    token_count = tokens.shape[0]
    own_rows = tokens.astype(jnp.float32)
    normed_own = (
        own_rows
        * lax.rsqrt(jnp.mean(own_rows * own_rows, axis=-1, keepdims=True) + EPSILON)
        * norm_gain
    ).astype(jnp.bfloat16)
    normed = gathered(normed_own)
    normed = normed.reshape(seq_count, proposals, -1).transpose(1, 0, 2)
    normed = normed.reshape(proposals * seq_count, -1)

    def project(weight):
        out = jnp.dot(normed, weight, preferred_element_type=jnp.float32)
        return out.reshape(proposals, seq_count, -1)

    gate_rows = project(gate_proj).astype(jnp.bfloat16)
    inner_rows = project(inner_proj).astype(jnp.bfloat16)
    write_rows = project(write_proj).astype(jnp.bfloat16)
    read_rows = project(read_proj).astype(jnp.bfloat16)
    first_head = device_rank * local_heads
    steps = lax.dynamic_slice_in_dim(project(step_proj), first_head, local_heads, 2)
    par = lax.dynamic_slice_in_dim(
        jnp.stack([step_bias, decay_log, skip_gain]), first_head, local_heads, 1
    )
    slab = lambda x: x.transpose(1, 0, 2)
    hist_inner, hist_write, hist_read = slab(inner_history), slab(write_history), slab(read_history)
    pieces = (write_rows, read_rows, hist_write, hist_read)
    group_span = lax.axis_size("kv") * lax.axis_size("tp") // GROUPS
    if group_span >= 2:
        pieces = tuple(lax.all_gather(x, "tp", axis=2, tiled=True) for x in pieces)
        kv_rank = lax.axis_index("kv")
        bit_count = (group_span // lax.axis_size("tp")).bit_length() - 1
        for bit in range(bit_count):
            partner = swapped(pieces, "kv", bit)
            lower = jnp.bitwise_and(jnp.right_shift(kv_rank, bit), 1) == 0
            pieces = tuple(
                jnp.where(
                    lower,
                    jnp.concatenate([mine, theirs], axis=2),
                    jnp.concatenate([theirs, mine], axis=2),
                )
                for mine, theirs in zip(pieces, partner)
            )
    write_rows, read_rows, hist_write, hist_read = pieces
    unscaled, squares, base_state = mix(
        device_rank,
        device_rank // group_span,
        accepted[:, None],
        steps,
        slab(last_steps),
        par,
        gate_rows,
        inner_rows,
        write_rows,
        read_rows,
        hist_inner,
        hist_write,
        hist_read,
        conv_inner,
        conv_write,
        conv_read,
        out_gain[None, :],
        saved_state.reshape(seq_count, local_heads * head_dim, -1),
    )
    base_state = base_state.reshape(saved_state.shape)
    unscaled = unscaled.transpose(1, 0, 2).reshape(seq_count * proposals, inner_cols)
    partial_value = jnp.dot(unscaled, out_proj, preferred_element_type=jnp.float32)
    squares = squares[:, :, 0].T.reshape(-1)
    square_total = lax.psum(squares, ("kv", "tp"))
    summed = lax.psum_scatter(partial_value, ("kv", "tp"), scatter_dimension=0, tiled=True)
    square_own = lax.dynamic_slice_in_dim(square_total, device_rank * token_count, token_count, 0)
    mixed = (summed * lax.rsqrt(square_own / out_gain.shape[0] + EPSILON)[:, None]).astype(jnp.bfloat16)
    return (mixed, base_state)


def solution(mesh):
    placed = (
        P(("dp", "kv", "tp"), None),
        P(),
        P(None, ("kv", "tp")),
        P(None, ("kv", "tp")),
        P(None, ("kv", "tp")),
        P(None, ("kv", "tp")),
        P(),
        P(),
        P(),
        P(),
        P(),
        P(),
        P(),
        P(),
        P(("kv", "tp"), None),
        P("dp", ("kv", "tp"), None, None),
        P("dp", None, ("kv", "tp")),
        P("dp", None, ("kv", "tp")),
        P("dp", None, ("kv", "tp")),
        P("dp", None, ("kv", "tp")),
        P("dp"),
    )
    return jax.shard_map(
        body,
        mesh=mesh,
        in_specs=placed,
        out_specs=(P(("dp", "kv", "tp"), None), P("dp", ("kv", "tp"), None, None)),
        check_vma=False,
    )
```

time: 171 us -> 115 us (0.67)
  matrix products: 63 us -> 9.97 us
  local copies, waits for them, and re-layouts: 34.5 us -> 4.64 us
  Pallas kernels: 0 us -> 22.1 us
  waiting for transfers between devices: 20.8 us -> 42.6 us
  other arithmetic: 18.6 us -> 5.41 us
  blocking collectives: 18.3 us -> 15.6 us
    dot_general x9 -> x5, matrix products: 60.9 us -> 7.86 us  [project(): out = jnp.dot(normed, weight, preferred_element_type=jnp.float32)]
    all_gather x1, waiting for transfers between devices: 0.02 us -> 22.6 us  [gathered(): return lax.all_gather(own, ('kv', 'tp'), axis=0, tiled=True)]
    pallas_call x0 -> x1, Pallas kernels: none -> 22.1 us  [mix(): pl.pallas_call(mix_kernel, grid_spec=pltpu.PrefetchScalarGridSpec(num_sca...]
    gather x7 -> x0, local copies, waits for them, and re-layouts: 11.3 us -> none  [current(): window = jnp.take_along_axis(history, window_rows[:, :, None], axis=1)]
    reshape x8 -> x3, local copies, waits for them, and re-layouts: 8.18 us -> 1.64 us  [the longest x1 1.46 us: body(): normed = normed.reshape(seq_count, proposals, -1).transpose(1, 0, 2)]
    convert_element_type x12 -> x2, other arithmetic: 8.09 us -> 1.69 us  [the longest x1 1.69 us: body(): (summed * lax.rsqrt(square_own / out_gain.shape[0] + EPSILON)[:, None]).a...]
    exp x4 -> x0, local copies, waits for them, and re-layouts: 4.17 us -> none  [the longest x2 2.79 us: body(): jnp.exp(cumulative)[..., None]]
    dynamic_slice x3 -> x2, local copies, waits for them, and re-layouts: 3.32 us -> 0.18 us  [the longest x1 0.11 us: body(): lax.dynamic_slice_in_dim(project(step_proj), first_head, local_heads, 2)]
  transfers between devices with their start and end apart: 2 -> 2, of which waited for: 1 -> 2; matrix products, arithmetic and copies ran while one was open for 17% -> 2% of each run, Pallas kernels for 0% -> 0%
where the time goes in v1:
time: 115 us
  waiting for transfers between devices  42.6 us (37%)
  Pallas kernels  22.1 us (19%)
  blocking collectives  15.6 us (14%)
  between operations  14.2 us (12%)
  matrix products  9.97 us (9%)
  other arithmetic  5.41 us (5%)
  local copies, waits for them, and re-layouts  4.64 us (4%)
    all_gather x1, waiting for transfers between devices, gathered(): return lax.all_gather(own, ('kv', 'tp'), axis=0, tiled=True)  22.6 us
    pallas_call x1, Pallas kernels, mix(): pl.pallas_call(mix_kernel, grid_spec=pltpu.PrefetchScalarGridSpec(num_sca...  22.1 us
    reduce_scatter x1, waiting for transfers between devices, body(): lax.psum_scatter(partial_value, ('kv', 'tp'), scatter_dimension=0, tiled=...  19.9 us
    psum x1, blocking collectives, body(): square_total = lax.psum(squares, ('kv', 'tp'))  15.6 us
    dot_general x5, matrix products, project(): out = jnp.dot(normed, weight, preferred_element_type=jnp.float32)  7.86 us
  transfers between devices with their start and end apart: 2, of which 2 were waited for; matrix products, arithmetic and copies ran while one was open for 2% of the time, Pallas kernels for 0%

profile of v1, /device:TPU:0, one launch (start us, length us, event | category | flops | bytes accessed | tf_op | source)
XLA Modules:
  0.0 114.6 jit_solution(10292113712729813921)
XLA Ops:
  7.2 1.2 %fusion.23 = f32[32]{0:T(128)S(1)} fusion(bf16[32,2048]{1,0:T(8,128)(2,1)} %param.21), kind=kLoop, calls=%fused_computation.23 | loop fusion | flops 196576 | bytes 131200 | tf_op jit(solution)/shard_map/reduce_sum | solution.py:261
  8.4 1.7 %fusion.25 = bf16[32,2048]{1,0:T(8,128)(2,1)} fusion(bf16[32,2048]{1,0:T(8,128)(2,1)} %param.21, f32[2048]{0:T(1024)} %param.22, f32[32]{0:T(128)S(1)} %add_rsqrt_fusion.1), kind=kLoop, calls=%fused_computation.25 | loop fusion | flops 262144 | bytes 270464 | tf_op jit(solution)/shard_map/convert_element_type | solution.py:263
  10.2 0.7 copy.29.acc_ref
  10.9 0.8 copy.28
  11.8 0.7 pad_maximum_fusion
  12.6 22.6 %all-gather.2.cloned.1.call-done = bf16[256,2048]{1,0:T(8,128)(2,1)} async-done(((bf16[32,2048]{1,0:T(8,128)(2,1)}), bf16[256,2048]{1,0:T(8,128)(2,1)}) %all-gather.2.cloned.1.call-update) | async-done | bytes 1048592 | tf_op jit(solution)/shard_map/all_gather | solution.py:224
  35.2 1.5 %reshape.82 = bf16[64,4,2048]{2,1,0:T(4,128)(2,1)S(1)} reshape(bf16[256,2048]{1,0:T(8,128)(2,1)} %all-gather.2.cloned.1.call-done) | data formatting | bytes 2097152 | tf_op jit(solution)/shard_map/reshape | solution.py:265
  36.7 2.4 %convolution_convert_fusion.read_ref = bf16[4,64,128]{2,1,0:T(8,128)(2,1)S(1)} fusion(bf16[64,4,2048]{2,1,0:T(4,128)(2,1)S(1)} %reshape.82, bf16[2048,128]{1,0:T(8,128)(2,1)} %param.26), kind=kOutput, calls=%fused_computation.6 | convolution fusion | flops 134250496 | bytes 1638400 | tf_op jit(solution)/shard_map/dot_general | solution.py:269
  39.1 2.5 %convolution_convert_fusion.1.write_ref = bf16[4,64,128]{2,1,0:T(8,128)(2,1)S(1)} fusion(bf16[64,4,2048]{2,1,0:T(4,128)(2,1)S(1)} %reshape.82, bf16[2048,128]{1,0:T(8,128)(2,1)} %param.25), kind=kOutput, calls=%fused_computation.7 | convolution fusion | flops 134250496 | bytes 1638400 | tf_op jit(solution)/shard_map/dot_general | solution.py:269
  41.5 1.2 %fusion.14 = f32[4,64,64]{2,1,0:T(8,128)S(1)} fusion(bf16[64,4,2048]{2,1,0:T(4,128)(2,1)S(1)} %reshape.82, bf16[2048,64]{0,1:T(8,128)(2,1)S(1)} %copy-done.10), kind=kOutput, calls=%fused_computation.12 | convolution fusion | flops 67108864 | bytes 1376256 | tf_op jit(solution)/shard_map/dot_general | solution.py:269
  42.8 0.1 constant_dynamic-slice_fusion.1.steps_ref
  42.9 0.9 fusion.7.inner_ref
  43.8 0.7 copy-done.9
  44.6 0.9 fusion.4.gate_ref
  45.6 22.1 %mix.1 = (bf16[4,64,512]{2,1,0:T(8,128)(2,1)S(1)}, f32[4,64,128]{2,1,0:T(8,128)S(1)}, f32[64,512,128]{2,1,0:T(8,128)}) custom-call(s32[2]{0:T(128)S(1)} %pad_add_fusion.rank_ref, s32[64,1]{1,0:T(8,128)S(1)} %copy.29.acc_ref, f32[4,64,8]{2,1,0:T(8,128)S(1)} %constant_dynamic-slice_fusion.1.steps_ref, f32[4,64,8]{2,1,0:T(8,128)S(1)} %bitcast.46, ...), custom_call_target="tpu_custom_call" | custom-call | tf_op jit(solution)/shard_map/mix/pallas_call | solution.py:182
  67.7 0.2 copy.30
  68.0 2.1 %fusion.31 = f32[256,2048]{1,0:T(8,128)} fusion(bf16[256,512]{1,0:T(8,128)(2,1)S(1)} %reshape.84, bf16[512,2048]{1,0:T(8,128)(2,1)S(1)} %copy-done), kind=kOutput, calls=%fused_computation.44 | convolution fusion | flops 536870912 | bytes 4456448 | tf_op jit(solution)/shard_map/dot_general | solution.py:323
  70.1 0.1 slice_reduce_fusion
  70.3 0.1 copy.31
  70.3 0.1 reshape.85
  70.5 15.6 %psum.7 = f32[256]{0:T(256)S(1)} all-reduce(f32[256]{0:T(256)S(1)} %reshape.85), channel_id=1, replica_groups=mesh['dp'=4,'kv'=4,'tp'=2] {'kv','tp'}, use_global_device_ids=true, to_apply=%region_2.3 | all-reduce | flops 256 | bytes 2048 | tf_op jit(solution)/shard_map/psum | solution.py:325
  86.1 0.1 add_rsqrt_fusion
  86.2 19.9 %reduce-scatter.2.cloned.1.call-done = f32[32,2048]{1,0:T(8,128)} async-done(((f32[256,2048]{1,0:T(8,128)}), f32[32,2048]{1,0:T(8,128)}) %reduce-scatter.2.cloned.1.call-update) | async-done | bytes 262160 | tf_op jit(solution)/shard_map/reduce_scatter | solution.py:326
  106.1 1.7 %multiply_convert_fusion = bf16[32,2048]{1,0:T(8,128)(2,1)} fusion(f32[32,2048]{1,0:T(8,128)} %reduce-scatter.2.cloned.1.call-done, f32[32]{0:T(128)S(1)} %add_rsqrt_fusion), kind=kLoop, calls=%fused_computation.27 | loop fusion | flops 131072 | bytes 393344 | tf_op jit(solution)/shard_map/convert_element_type | solution.py:328
  (31 shorter events, 0.5 us)
Async XLA Ops:
  7.2 60.8 %copy-start = (bf16[512,2048]{1,0:T(8,128)(2,1)S(1)}, bf16[512,2048]{1,0:T(8,128)(2,1)}, u32[]{:S(2)}) copy-start(bf16[512,2048]{1,0:T(8,128)(2,1)} %param.35) | copy-start | bytes 6291460
  7.2 28.0 %all-gather.2.cloned.1.call-start = ((), (), s32[]{:S(2)}) async-start(), calls=%async_computation.1 | async-start | bytes 1179648 | tf_op jit(solution)/shard_map/all_gather | solution.py:224
  10.1 96.0 %reduce-scatter.2.cloned.1.call-start = ((), (), s32[]{:S(2)}) async-start(), calls=%async_computation.2 | async-start | bytes 2359296 | tf_op jit(solution)/shard_map/reduce_scatter | solution.py:326
  36.7 4.9 %copy-start.10 = (bf16[2048,64]{0,1:T(8,128)(2,1)S(1)}, bf16[2048,64]{0,1:T(8,128)(2,1)}, u32[]{:S(2)}) copy-start(bf16[2048,64]{0,1:T(8,128)(2,1)} %param.27) | copy-start | bytes 786436
  39.1 3.8 %copy-start.8 = (bf16[2048,512]{1,0:T(8,128)(2,1)S(1)}, bf16[2048,512]{1,0:T(8,128)(2,1)}, u32[]{:S(2)}) copy-start(bf16[2048,512]{1,0:T(8,128)(2,1)} %param.24) | copy-start | bytes 6291460
  42.9 1.6 %copy-start.9 = (bf16[2048,512]{1,0:T(8,128)(2,1)S(1)}, bf16[2048,512]{1,0:T(8,128)(2,1)}, u32[]{:S(2)}) copy-start(bf16[2048,512]{1,0:T(8,128)(2,1)} %param.23) | copy-start | bytes 6291460
  44.5 1.0 copy-start.1
  44.5 1.0 copy-start.2
  44.5 1.1 copy-start.3
  44.5 1.1 copy-start.4
  44.5 1.1 copy-start.5
  44.5 1.1 copy-start.6
  44.5 1.1 copy-start.7
Sparse Core Ops, SparseCore 0:
  10.2 24.9 all-gather.1
  70.3 35.7 reduce-scatter.1

commit v2 on v1

--- a/solution.py
+++ b/solution.py
@@ -220,8 +220,286 @@
     )
 
 
+MESH = pl.DeviceIdType.MESH
+CHUNKS = 2
+
+
+def remote(src, dst, send, recv, where):
+    return pltpu.make_async_remote_copy(
+        src_ref=src, dst_ref=dst, send_sem=send, recv_sem=recv, device_id=where, device_id_type=MESH
+    )
+
+
+def gather_kernel(n, own_ref, out_ref, rs, rr, ls, lr, fs, fr, local_sem):
+    k = lax.axis_index("kv")
+    t = lax.axis_index("tp")
+    right = {"kv": lax.rem(k + 1, n)}
+    left = {"kv": lax.rem(k + n - 1, n)}
+    partner = {"tp": 1 - t}
+    span = own_ref.shape[1] // CHUNKS
+    barrier = pltpu.get_barrier_semaphore()
+    pl.semaphore_signal(barrier, inc=1, device_id=partner, device_id_type=MESH)
+
+    @pl.when(k < n - 1)
+    def _():
+        pl.semaphore_signal(barrier, inc=1, device_id=right, device_id_type=MESH)
+
+    @pl.when(k > 0)
+    def _():
+        pl.semaphore_signal(barrier, inc=1, device_id=left, device_id_type=MESH)
+
+    inner = (k > 0) & (k < n - 1)
+
+    @pl.when(inner)
+    def _():
+        pl.semaphore_wait(barrier, 3)
+
+    @pl.when(jnp.logical_not(inner))
+    def _():
+        pl.semaphore_wait(barrier, 2)
+
+    def view(j, c):
+        return out_ref.at[j, t, :, pl.ds(c * span, span)]
+
+    def own(c):
+        return own_ref.at[:, pl.ds(c * span, span)]
+
+    def to_right(s, c):
+        j = jnp.maximum(k - s, 0)
+        return remote(own(c) if s == 0 else view(j, c), view(j, c), rs.at[s, c], rr.at[s, c], right)
+
+    def to_left(s, c):
+        j = jnp.minimum(k + s, n - 1)
+        return remote(own(c) if s == 0 else view(j, c), view(j, c), ls.at[s, c], lr.at[s, c], left)
+
+    def across(j, c, mine=False):
+        return remote(own(c) if mine else view(j, c), view(j, c), fs.at[j, c], fr.at[j, c], partner)
+
+    for s in range(n - 1):
+        for c in range(CHUNKS):
+            if s > 0:
+                @pl.when(k - s >= 0)
+                def _():
+                    to_right(s - 1, c).wait_recv()
+
+                @pl.when(k + s < n)
+                def _():
+                    to_left(s - 1, c).wait_recv()
+
+            @pl.when((k - s >= 0) & (k < n - 1))
+            def _():
+                to_right(s, c).start()
+
+            @pl.when((k + s < n) & (k > 0))
+            def _():
+                to_left(s, c).start()
+
+            if s == 0:
+                across(k, c, True).start()
+            else:
+                @pl.when(k - s >= 0)
+                def _():
+                    across(k - s, c).start()
+
+                @pl.when(k + s < n)
+                def _():
+                    across(k + s, c).start()
+        if s == 0:
+            local = pltpu.make_async_copy(own_ref, out_ref.at[k, t], local_sem)
+            local.start()
+            local.wait()
+    s = n - 1
+    for c in range(CHUNKS):
+        @pl.when(k - s >= 0)
+        def _():
+            to_right(s - 1, c).wait_recv()
+            across(k - s, c).start()
+
+        @pl.when(k + s < n)
+        def _():
+            to_left(s - 1, c).wait_recv()
+            across(k + s, c).start()
+    for s in range(n - 1):
+        for c in range(CHUNKS):
+            @pl.when((k - s >= 0) & (k < n - 1))
+            def _():
+                to_right(s, c).wait_send()
+
+            @pl.when((k + s < n) & (k > 0))
+            def _():
+                to_left(s, c).wait_send()
+    for j in range(n):
+        for c in range(CHUNKS):
+            across(j, c).wait_send()
+            remote(
+                out_ref.at[j, 1 - t, :, pl.ds(c * span, span)],
+                out_ref.at[j, 1 - t, :, pl.ds(c * span, span)],
+                fs.at[j, c],
+                fr.at[j, c],
+                partner,
+            ).wait_recv()
+
+
 def gathered(own):
-    return lax.all_gather(own, ("kv", "tp"), axis=0, tiled=True)
+    n = lax.axis_size("kv")
+    rows, cols = own.shape
+    dma = pltpu.SemaphoreType.DMA
+    out = pl.pallas_call(
+        functools.partial(gather_kernel, n),
+        out_shape=jax.ShapeDtypeStruct((n, 2, rows, cols), own.dtype),
+        in_specs=[pl.BlockSpec(memory_space=pltpu.VMEM)],
+        out_specs=pl.BlockSpec(memory_space=pltpu.VMEM),
+        scratch_shapes=[dma((n - 1, CHUNKS))] * 4 + [dma((n, CHUNKS))] * 2 + [dma],
+        compiler_params=pltpu.CompilerParams(
+            collective_id=0, has_side_effects=True, vmem_limit_bytes=32 * 1024 * 1024
+        ),
+        name="gather",
+    )(own)
+    return out.reshape(n * 2 * rows, cols)
+
+
+def scatter_kernel(
+    n, part, sq, out, sqs, pbuf, rbuf, lbuf, rout, lout, ps, pr, rs, rr, ls, lr, ss, sr
+):
+    f32 = jnp.float32
+    k = lax.axis_index("kv")
+    t = lax.axis_index("tp")
+    rank = k * 2 + t
+    ranks = n * 2
+    right = {"kv": lax.rem(k + 1, n)}
+    left = {"kv": lax.rem(k + n - 1, n)}
+    partner = {"tp": 1 - t}
+    span = part.shape[3] // CHUNKS
+    barrier = pltpu.get_barrier_semaphore()
+
+    def peer(o):
+        p = lax.rem(rank + o, ranks)
+        return {"kv": p // 2, "tp": lax.rem(p, 2)}
+
+    for o in range(1, ranks):
+        pl.semaphore_signal(barrier, inc=1, device_id=peer(o), device_id_type=MESH)
+    pl.semaphore_wait(barrier, ranks - 1)
+
+    def cut(c):
+        return pl.ds(c * span, span)
+
+    def across(j, c):
+        return remote(
+            part.at[j, 1 - t, :, cut(c)], pbuf.at[j, :, cut(c)], ps.at[j, c], pr.at[j, c], partner
+        )
+
+    def to_right(d, c):
+        return remote(
+            rout.at[d, :, cut(c)], rbuf.at[d, :, cut(c)], rs.at[d, c], rr.at[d, c], right
+        )
+
+    def to_left(d, c):
+        return remote(lout.at[d, :, cut(c)], lbuf.at[d, :, cut(c)], ls.at[d, c], lr.at[d, c], left)
+
+    def square(o):
+        p = lax.rem(rank + o, ranks)
+        return remote(sq.at[p], sqs.at[rank], ss.at[o], sr.at[o], peer(o))
+
+    order = []
+    for i in range(n):
+        for j in (n - 1 - i, i):
+            if j not in order:
+                order.append(j)
+    for j in order:
+        for c in range(CHUNKS):
+            across(j, c).start()
+    for o in range(1, ranks):
+        square(o).start()
+    sqs[rank] = sq[rank]
+
+    def pair(j, c):
+        across(j, c).wait_recv()
+        return part[j, t, :, cut(c)].astype(f32) + pbuf[j, :, cut(c)].astype(f32)
+
+    for i in range(n - 1):
+        for c in range(CHUNKS):
+            d = n - 1 - i
+
+            @pl.when((k < d) & (k == 0))
+            def _():
+                rout[d, :, cut(c)] = pair(d, c).astype(rout.dtype)
+                to_right(d, c).start()
+
+            @pl.when((k < d) & (k > 0))
+            def _():
+                value = pair(d, c)
+                to_right(d, c).wait_recv()
+                rout[d, :, cut(c)] = (value + rbuf[d, :, cut(c)].astype(f32)).astype(rout.dtype)
+                to_right(d, c).start()
+
+            @pl.when((k > i) & (k == n - 1))
+            def _():
+                lout[i, :, cut(c)] = pair(i, c).astype(lout.dtype)
+                to_left(i, c).start()
+
+            @pl.when((k > i) & (k < n - 1))
+            def _():
+                value = pair(i, c)
+                to_left(i, c).wait_recv()
+                lout[i, :, cut(c)] = (value + lbuf[i, :, cut(c)].astype(f32)).astype(lout.dtype)
+                to_left(i, c).start()
+
+    for c in range(CHUNKS):
+        out[:, cut(c)] = pair(k, c)
+
+        @pl.when(k > 0)
+        def _():
+            to_right(k, c).wait_recv()
+            out[:, cut(c)] += rbuf[k, :, cut(c)].astype(f32)
+
+        @pl.when(k < n - 1)
+        def _():
+            to_left(k, c).wait_recv()
+            out[:, cut(c)] += lbuf[k, :, cut(c)].astype(f32)
+
+    for j in range(n):
+        for c in range(CHUNKS):
+            across(j, c).wait_send()
+
+            @pl.when(k < j)
+            def _():
+                to_right(j, c).wait_send()
+
+            @pl.when(k > j)
+            def _():
+                to_left(j, c).wait_send()
+    for o in range(1, ranks):
+        square(o).wait_send()
+        source = lax.rem(rank + ranks - o, ranks)
+        remote(sq.at[rank], sqs.at[source], ss.at[o], sr.at[o], peer(o)).wait_recv()
+
+
+def scattered(partial_value, squares):
+    n = lax.axis_size("kv")
+    ranks = n * 2
+    rows = partial_value.shape[0] // ranks
+    cols = partial_value.shape[1]
+    squares = jnp.pad(squares.reshape(ranks, 1, rows), ((0, 0), (0, 7), (0, 128 - rows)))
+    dma = pltpu.SemaphoreType.DMA
+    vmem = pl.BlockSpec(memory_space=pltpu.VMEM)
+    kind = partial_value.dtype
+    summed, sqs = pl.pallas_call(
+        functools.partial(scatter_kernel, n),
+        out_shape=[
+            jax.ShapeDtypeStruct((rows, cols), jnp.float32),
+            jax.ShapeDtypeStruct(squares.shape, jnp.float32),
+        ],
+        in_specs=[vmem, vmem],
+        out_specs=[vmem, vmem],
+        scratch_shapes=[pltpu.VMEM((n, rows, cols), kind)] * 5
+        + [dma((n, CHUNKS))] * 6
+        + [dma((ranks,))] * 2,
+        compiler_params=pltpu.CompilerParams(
+            collective_id=1, has_side_effects=True, vmem_limit_bytes=32 * 1024 * 1024
+        ),
+        name="scatter",
+    )(partial_value.reshape(n, 2, rows, cols), squares)
+    return summed, jnp.sum(sqs[:, 0, :rows], axis=0)
 
 
 def body(
@@ -322,9 +600,7 @@
     unscaled = unscaled.transpose(1, 0, 2).reshape(seq_count * proposals, inner_cols)
     partial_value = jnp.dot(unscaled, out_proj, preferred_element_type=jnp.float32)
     squares = squares[:, :, 0].T.reshape(-1)
-    square_total = lax.psum(squares, ("kv", "tp"))
-    summed = lax.psum_scatter(partial_value, ("kv", "tp"), scatter_dimension=0, tiled=True)
-    square_own = lax.dynamic_slice_in_dim(square_total, device_rank * token_count, token_count, 0)
+    summed, square_own = scattered(partial_value.astype(jnp.bfloat16), squares)
     mixed = (summed * lax.rsqrt(square_own / out_gain.shape[0] + EPSILON)[:, None]).astype(jnp.bfloat16)
     return (mixed, base_state)
 

time: 115 us -> 81.1 us (0.71)
  waiting for transfers between devices: 42.6 us -> 0 us
  Pallas kernels: 22.1 us -> 62.4 us
  blocking collectives: 15.6 us -> 0 us
  between operations: 14.2 us -> 0.82 us
  other arithmetic: 5.41 us -> 3.76 us
    pallas_call x0 -> x2, Pallas kernels: none -> 40.3 us  [the longest x1 23.9 us: scattered(): pl.pallas_call(functools.partial(scatter_kernel, n), out_shape=[jax.Shape...]
    all_gather x1 -> x0, waiting for transfers between devices: 22.6 us -> none  [gathered(): return lax.all_gather(own, ('kv', 'tp'), axis=0, tiled=True)]
    reduce_scatter x1 -> x0, waiting for transfers between devices: 19.9 us -> none  [body(): lax.psum_scatter(partial_value, ('kv', 'tp'), scatter_dimension=0, tiled=...]
    psum x1 -> x0, blocking collectives: 15.6 us -> none  [body(): square_total = lax.psum(squares, ('kv', 'tp'))]
    reshape x2 -> x0, local copies, waits for them, and re-layouts: 1.57 us -> none  [the longest x1 1.46 us: body(): normed = normed.reshape(seq_count, proposals, -1).transpose(1, 0, 2)]
    dot_general x1, matrix products: 2.1 us -> 0.71 us  [body(): jnp.dot(unscaled, out_proj, preferred_element_type=jnp.float32)]
    another operation x0 -> x2, local copies, waits for them, and re-layouts: none -> 1.29 us  [the longest x1 1.21 us: body(): normed = normed.reshape(seq_count, proposals, -1).transpose(1, 0, 2)]
  transfers between devices with their start and end apart: 2 -> 0, of which waited for: 2 -> 0; matrix products, arithmetic and copies ran while one was open for 2% -> 0% of each run, Pallas kernels for 0% -> 0%
where the time goes in v2:
time: 81.1 us; the launch traced here: 80.5 us
  Pallas kernels  62.4 us (77%)
  matrix products  9.22 us (11%)
  local copies, waits for them, and re-layouts  4.37 us (5%)
  other arithmetic  3.76 us (5%)
  between operations  0.82 us (1%)
    pallas_call x1, Pallas kernels, scattered(): pl.pallas_call(functools.partial(scatter_kernel, n), out_shape=[jax.Shape...  23.9 us
    pallas_call x1, Pallas kernels, mix(): pl.pallas_call(mix_kernel, grid_spec=pltpu.PrefetchScalarGridSpec(num_sca...  22.1 us
    pallas_call x1, Pallas kernels, gathered(): pl.pallas_call(functools.partial(gather_kernel, n), out_shape=jax.ShapeDt...  16.4 us
    dot_general x5, matrix products, project(): out = jnp.dot(normed, weight, preferred_element_type=jnp.float32)  8.51 us
    unnamed x25, local copies, waits for them, and re-layouts  1.66 us

profile of v2, /device:TPU:0, one launch (start us, length us, event | category | flops | bytes accessed | tf_op | source)
XLA Modules:
  0.0 80.5 jit_solution(8596318155396252544)
XLA Ops:
  0.7 0.1 pad_add_fusion.rank_ref
  0.7 1.2 %fusion.23 = f32[32]{0:T(128)S(1)} fusion(bf16[32,2048]{1,0:T(8,128)(2,1)} %param.21), kind=kLoop, calls=%fused_computation.24 | loop fusion | flops 196576 | bytes 131200 | tf_op jit(solution)/shard_map/reduce_sum | solution.py:539
  1.9 0.7 pad_maximum_fusion
  2.6 0.1 constant_dynamic-slice_fusion.par_ref
  2.7 0.7 copy.31.acc_ref
  3.4 1.0 %fusion.25.own_ref = bf16[32,2048]{1,0:T(8,128)(2,1)S(1)} fusion(bf16[32,2048]{1,0:T(8,128)(2,1)} %param.21, f32[2048]{0:T(1024)} %param.22, f32[32]{0:T(128)S(1)} %add_rsqrt_fusion.1), kind=kLoop, calls=%fused_computation.26 | loop fusion | flops 262144 | bytes 270464 | tf_op jit(solution)/shard_map/convert_element_type | solution.py:541
  4.5 0.8 %copy.30 = f32[64,4,8]{2,0,1:T(8,128)S(1)} copy(f32[64,4,8]{0,2,1:T(8,128)} %param.40) | data formatting | bytes 16384 | tf_op args[19]
  5.3 16.4 %gather.1 = bf16[4,2,32,2048]{3,2,1,0:T(8,128)(2,1)S(1)} custom-call(bf16[32,2048]{1,0:T(8,128)(2,1)S(1)} %fusion.25.own_ref), custom_call_target="tpu_custom_call" | custom-call | tf_op jit(solution)/shard_map/gather/pallas_call | solution.py:347
  21.6 1.2 %reshape_reshape.6 = bf16[64,4,2048]{2,1,0:T(4,128)(2,1)} reshape(bf16[4,2,32,2048]{3,2,1,0:T(8,128)(2,1)S(1)} %gather.1) | data formatting | bytes 2097152 | tf_op jit(solution)/shard_map/reshape;reshape | solution.py:543
  22.8 2.7 %convolution_convert_fusion.1.read_ref = bf16[4,64,128]{2,1,0:T(8,128)(2,1)S(1)} fusion(bf16[64,4,2048]{2,1,0:T(4,128)(2,1)} %reshape_reshape.6, bf16[2048,128]{1,0:T(8,128)(2,1)} %param.26), kind=kOutput, calls=%fused_computation.7 | convolution fusion | flops 134250496 | bytes 1638400 | tf_op jit(solution)/shard_map/dot_general | solution.py:547
  25.6 2.8 %convolution_convert_fusion.2.write_ref = bf16[4,64,128]{2,1,0:T(8,128)(2,1)S(1)} fusion(bf16[64,4,2048]{2,1,0:T(4,128)(2,1)} %reshape_reshape.6, bf16[2048,128]{1,0:T(8,128)(2,1)} %param.25), kind=kOutput, calls=%fused_computation.8 | convolution fusion | flops 134250496 | bytes 1638400 | tf_op jit(solution)/shard_map/dot_general | solution.py:547
  28.4 1.2 %fusion.14 = f32[4,64,64]{2,1,0:T(8,128)S(1)} fusion(bf16[64,4,2048]{2,1,0:T(4,128)(2,1)S(1)} %copy-done.8, bf16[2048,64]{0,1:T(8,128)(2,1)S(1)} %copy-done.11), kind=kOutput, calls=%fused_computation.13 | convolution fusion | flops 67108864 | bytes 1376256 | tf_op jit(solution)/shard_map/dot_general | solution.py:547
  29.6 0.1 constant_dynamic-slice_fusion.1.steps_ref
  29.7 0.9 %fusion.7.inner_ref = bf16[4,64,512]{2,1,0:T(8,128)(2,1)S(1)} fusion(bf16[2048,512]{1,0:T(8,128)(2,1)S(1)} %copy-done.9, bf16[64,4,2048]{2,1,0:T(4,128)(2,1)S(1)} %copy-done.8), kind=kOutput, calls=%fused_computation.6 | convolution fusion | flops 537001984 | bytes 3407872 | tf_op jit(solution)/shard_map/dot_general | solution.py:547
  30.6 0.7 copy-done.10
  31.4 0.9 %fusion.4.gate_ref = bf16[4,64,512]{2,1,0:T(8,128)(2,1)S(1)} fusion(bf16[2048,512]{1,0:T(8,128)(2,1)S(1)} %copy-done.10, bf16[64,4,2048]{2,1,0:T(4,128)(2,1)S(1)} %copy-done.8), kind=kOutput, calls=%fused_computation.5 | convolution fusion | flops 537001984 | bytes 3407872 | tf_op jit(solution)/shard_map/dot_general | solution.py:547
  32.4 22.1 %mix.1 = (bf16[4,64,512]{2,1,0:T(8,128)(2,1)S(1)}, f32[4,64,128]{2,1,0:T(8,128)S(1)}, f32[64,512,128]{2,1,0:T(8,128)}) custom-call(s32[2]{0:T(128)S(1)} %pad_add_fusion.rank_ref, s32[64,1]{1,0:T(8,128)S(1)} %copy.31.acc_ref, f32[4,64,8]{2,1,0:T(8,128)S(1)} %constant_dynamic-slice_fusion.1.steps_ref, f32[4,64,8]{2,1,0:T(8,128)S(1)} %bitcast.51, ...), custom_call_target="tpu_custom_call" | custom-call | tf_op jit(solution)/shard_map/mix/pallas_call | solution.py:182
  54.5 0.2 copy.32
  54.8 0.1 slice_reduce_fusion
  54.9 0.1 copy.33
  55.0 0.1 reshape_reshape.7
  55.1 0.7 convolution_convert_fusion
  55.8 23.9 %scatter.1 = (f32[32,2048]{1,0:T(8,128)S(1)}, f32[8,8,128]{2,1,0:T(8,128)S(1)}) custom-call(bf16[4,2,32,2048]{3,2,1,0:T(8,128)(2,1)S(1)} %bitcast.50, f32[8,8,128]{2,1,0:T(8,128)S(1)} %pad.4.sq), custom_call_target="tpu_custom_call" | custom-call | tf_op jit(solution)/shard_map/scatter/pallas_call | solution.py:486
  79.8 0.7 multiply_convert_fusion
  (30 shorter events, 0.3 us)
Async XLA Ops:
  0.6 54.5 %copy-start = (bf16[512,2048]{1,0:T(8,128)(2,1)S(1)}, bf16[512,2048]{1,0:T(8,128)(2,1)}, u32[]{:S(2)}) copy-start(bf16[512,2048]{1,0:T(8,128)(2,1)} %param.35) | copy-start | bytes 6291460
  22.8 5.5 %copy-start.8 = (bf16[64,4,2048]{2,1,0:T(4,128)(2,1)S(1)}, bf16[64,4,2048]{2,1,0:T(4,128)(2,1)}, u32[]{:S(2)}) copy-start(bf16[64,4,2048]{2,1,0:T(4,128)(2,1)} %reshape_reshape.6) | copy-start | bytes 3145732
  22.8 5.5 %copy-start.11 = (bf16[2048,64]{0,1:T(8,128)(2,1)S(1)}, bf16[2048,64]{0,1:T(8,128)(2,1)}, u32[]{:S(2)}) copy-start(bf16[2048,64]{0,1:T(8,128)(2,1)} %param.27) | copy-start | bytes 786436
  25.6 4.1 %copy-start.9 = (bf16[2048,512]{1,0:T(8,128)(2,1)S(1)}, bf16[2048,512]{1,0:T(8,128)(2,1)}, u32[]{:S(2)}) copy-start(bf16[2048,512]{1,0:T(8,128)(2,1)} %param.24) | copy-start | bytes 6291460
  29.7 1.6 %copy-start.10 = (bf16[2048,512]{1,0:T(8,128)(2,1)S(1)}, bf16[2048,512]{1,0:T(8,128)(2,1)}, u32[]{:S(2)}) copy-start(bf16[2048,512]{1,0:T(8,128)(2,1)} %param.23) | copy-start | bytes 6291460
  31.3 1.0 %copy-start.1 = (bf16[64,7,512]{2,0,1:T(8,128)(2,1)S(1)}, bf16[64,7,512]{2,0,1:T(8,128)(2,1)}, u32[]{:S(2)}) copy-start(bf16[64,7,512]{2,0,1:T(8,128)(2,1)} %param.37) | copy-start | bytes 1376260
  31.3 1.0 %copy-start.2 = (bf16[64,7,128]{2,0,1:T(8,128)(2,1)S(1)}, bf16[64,7,128]{2,0,1:T(8,128)(2,1)}, u32[]{:S(2)}) copy-start(bf16[64,7,128]{2,0,1:T(8,128)(2,1)} %param.38) | copy-start | bytes 344068
  31.3 1.1 %copy-start.3 = (bf16[64,7,128]{2,0,1:T(8,128)(2,1)S(1)}, bf16[64,7,128]{2,0,1:T(8,128)(2,1)}, u32[]{:S(2)}) copy-start(bf16[64,7,128]{2,0,1:T(8,128)(2,1)} %param.39) | copy-start | bytes 344068
  31.3 1.1 %copy-start.4 = (bf16[4,4096]{1,0:T(4,128)(2,1)S(1)}, bf16[4,4096]{1,0:T(4,128)(2,1)}, u32[]{:S(2)}) copy-start(bf16[4,4096]{1,0:T(4,128)(2,1)} %taps_inner_ref.1) | copy-start | bytes 98308
  31.3 1.1 %copy-start.5 = (f32[4096]{0:T(1024)S(1)}, f32[4096]{0:T(1024)}, u32[]{:S(2)}) copy-start(f32[4096]{0:T(1024)} %param.34) | copy-start | bytes 49156
  31.3 1.1 %copy-start.6 = (bf16[4,1024]{1,0:T(4,128)(2,1)S(1)}, bf16[4,1024]{1,0:T(4,128)(2,1)}, u32[]{:S(2)}) copy-start(bf16[4,1024]{1,0:T(4,128)(2,1)} %taps_write_ref.1) | copy-start | bytes 24580
  31.3 1.1 %copy-start.7 = (bf16[4,1024]{1,0:T(4,128)(2,1)S(1)}, bf16[4,1024]{1,0:T(4,128)(2,1)}, u32[]{:S(2)}) copy-start(bf16[4,1024]{1,0:T(4,128)(2,1)} %taps_read_ref.1) | copy-start | bytes 24580

commit v3 on v2

--- a/solution.py
+++ b/solution.py
@@ -44,7 +44,7 @@
 ):
     f32 = jnp.float32
     props = steps_ref.shape[0]
-    heads = steps_ref.shape[2]
+    heads = last_ref.shape[2]
     cols = inner_ref.shape[2]
     states = write_ref.shape[2]
     head_dim = cols // heads
@@ -57,6 +57,8 @@
 
     def slabs(ref):
         return [ref[k].astype(f32) for k in range(ref.shape[0])]
+
+    round_bf = lambda x: x.astype(jnp.bfloat16).astype(f32)
 
     def conv(rows, taps_ref):
         taps = taps_ref[...].astype(f32)
@@ -76,13 +78,12 @@
             for v in range(1, hist - width + 2):
                 r = jnp.where(where_at == v, h[k + v], r)
             rows.append(r)
-        return rows + slabs(new_ref)
+        return rows + [round_bf(x) for x in slabs(new_ref)]
 
     h_inner = slabs(hist_inner_ref)
     inner_old = conv(h_inner, taps_inner_ref)
     inner_new = conv(current(h_inner, inner_ref), taps_inner_ref)
     h_write = slabs(hist_write_ref)
-    round_bf = lambda x: x.astype(jnp.bfloat16).astype(f32)
     write_old = [round_bf(x) for x in conv(h_write, taps_write_ref)]
     write_new = [round_bf(x) for x in conv(current(h_write, write_ref), taps_write_ref)]
     read_new = [round_bf(x) for x in conv(current(slabs(hist_read_ref), read_ref), taps_read_ref)]
@@ -101,7 +102,7 @@
     decay = jnp.exp(tail)
     step = []
     for t in range(props):
-        x = steps_ref[t] + bias
+        x = steps_ref[t][:, :heads] + bias
         step.append(jnp.maximum(x, 0.0) + jnp.log1p(jnp.exp(-jnp.abs(x))))
     cums = []
     for t in range(props):
@@ -163,8 +164,8 @@
         un_ref[i] = (g * gain_ref[...]).astype(un_ref.dtype)
 
 
-def mix(rank, group, acc, steps, last, par, gate, inner, write, read, hi, hw, hr, ci, cw, cr, gain, state):
-    props, seqs, heads = steps.shape
+def mix(rank, group, acc, last, par, gate, inner, small, hi, hw, hr, ci, cw, cr, gain, state):
+    props, seqs, heads = last.shape
     cols, states = state.shape[1], state.shape[2]
     expand = (jnp.arange(cols)[None, :] // (cols // heads) == jnp.arange(heads)[:, None]).astype(
         jnp.float32
@@ -174,6 +175,9 @@
 
     def slab(lead, last_dim):
         return pl.BlockSpec((lead, BLOCK, last_dim), lambda g, r: (0, g, 0))
+
+    def piece(which):
+        return pl.BlockSpec((props, BLOCK, states), lambda g, r: (0, g, which))
 
     def own(rows, last_dim, which):
         return pl.BlockSpec((rows, last_dim), lambda g, r: (0, r[which]))
@@ -186,13 +190,13 @@
             grid=(seqs // BLOCK,),
             in_specs=[
                 pl.BlockSpec((BLOCK, 1), lambda g, r: (g, 0)),
-                slab(props, heads),
+                piece(2),
                 slab(props, heads),
                 pl.BlockSpec(par.shape, lambda g, r: (0, 0)),
                 slab(props, cols),
                 slab(props, cols),
-                slab(props, states),
-                slab(props, states),
+                piece(0),
+                piece(1),
                 slab(hist, cols),
                 slab(hist, states),
                 slab(hist, states),
@@ -216,7 +220,7 @@
         name="mix",
     )(
         jnp.stack([rank, group]).astype(jnp.int32),
-        acc, steps, last, par, gate, inner, write, read, hi, hw, hr, ci, cw, cr, gain, expand, state,
+        acc, small, last, par, gate, inner, small, small, hi, hw, hr, ci, cw, cr, gain, expand, state,
     )
 
 
@@ -400,12 +404,9 @@
         p = lax.rem(rank + o, ranks)
         return remote(sq.at[p], sqs.at[rank], ss.at[o], sr.at[o], peer(o))
 
-    order = []
+    low = k < n // 2
     for i in range(n):
-        for j in (n - 1 - i, i):
-            if j not in order:
-                order.append(j)
-    for j in order:
+        j = jnp.where(low, n - 1 - i, i)
         for c in range(CHUNKS):
             across(j, c).start()
     for o in range(1, ranks):
@@ -416,33 +417,45 @@
         across(j, c).wait_recv()
         return part[j, t, :, cut(c)].astype(f32) + pbuf[j, :, cut(c)].astype(f32)
 
-    for i in range(n - 1):
-        for c in range(CHUNKS):
-            d = n - 1 - i
-
-            @pl.when((k < d) & (k == 0))
-            def _():
-                rout[d, :, cut(c)] = pair(d, c).astype(rout.dtype)
-                to_right(d, c).start()
-
-            @pl.when((k < d) & (k > 0))
-            def _():
-                value = pair(d, c)
-                to_right(d, c).wait_recv()
-                rout[d, :, cut(c)] = (value + rbuf[d, :, cut(c)].astype(f32)).astype(rout.dtype)
-                to_right(d, c).start()
-
-            @pl.when((k > i) & (k == n - 1))
-            def _():
-                lout[i, :, cut(c)] = pair(i, c).astype(lout.dtype)
-                to_left(i, c).start()
-
-            @pl.when((k > i) & (k < n - 1))
-            def _():
-                value = pair(i, c)
-                to_left(i, c).wait_recv()
-                lout[i, :, cut(c)] = (value + lbuf[i, :, cut(c)].astype(f32)).astype(lout.dtype)
-                to_left(i, c).start()
+    def rightward():
+        for d in range(n - 1, 0, -1):
+            for c in range(CHUNKS):
+                @pl.when((k < d) & (k == 0))
+                def _():
+                    rout[d, :, cut(c)] = pair(d, c).astype(rout.dtype)
+                    to_right(d, c).start()
+
+                @pl.when((k < d) & (k > 0))
+                def _():
+                    value = pair(d, c)
+                    to_right(d, c).wait_recv()
+                    rout[d, :, cut(c)] = (value + rbuf[d, :, cut(c)].astype(f32)).astype(rout.dtype)
+                    to_right(d, c).start()
+
+    def leftward():
+        for d in range(n - 1):
+            for c in range(CHUNKS):
+                @pl.when((k > d) & (k == n - 1))
+                def _():
+                    lout[d, :, cut(c)] = pair(d, c).astype(lout.dtype)
+                    to_left(d, c).start()
+
+                @pl.when((k > d) & (k < n - 1))
+                def _():
+                    value = pair(d, c)
+                    to_left(d, c).wait_recv()
+                    lout[d, :, cut(c)] = (value + lbuf[d, :, cut(c)].astype(f32)).astype(lout.dtype)
+                    to_left(d, c).start()
+
+    @pl.when(k < n // 2)
+    def _():
+        rightward()
+        leftward()
+
+    @pl.when(k >= n // 2)
+    def _():
+        leftward()
+        rightward()
 
     for c in range(CHUNKS):
         out[:, cut(c)] = pair(k, c)
@@ -549,18 +562,22 @@
 
     gate_rows = project(gate_proj).astype(jnp.bfloat16)
     inner_rows = project(inner_proj).astype(jnp.bfloat16)
-    write_rows = project(write_proj).astype(jnp.bfloat16)
-    read_rows = project(read_proj).astype(jnp.bfloat16)
     first_head = device_rank * local_heads
-    steps = lax.dynamic_slice_in_dim(project(step_proj), first_head, local_heads, 2)
+    state_cols = write_proj.shape[1]
+    states = saved_state.shape[3]
+    step_local = lax.dynamic_slice_in_dim(step_proj, first_head, local_heads, 1)
+    step_local = jnp.pad(step_local, ((0, 0), (0, states - local_heads)))
+    small = project(jnp.concatenate([write_proj, read_proj, step_local], axis=1))
     par = lax.dynamic_slice_in_dim(
         jnp.stack([step_bias, decay_log, skip_gain]), first_head, local_heads, 1
     )
     slab = lambda x: x.transpose(1, 0, 2)
     hist_inner, hist_write, hist_read = slab(inner_history), slab(write_history), slab(read_history)
-    pieces = (write_rows, read_rows, hist_write, hist_read)
     group_span = lax.axis_size("kv") * lax.axis_size("tp") // GROUPS
     if group_span >= 2:
+        write_rows = small[:, :, :state_cols].astype(jnp.bfloat16)
+        read_rows = small[:, :, state_cols : 2 * state_cols].astype(jnp.bfloat16)
+        pieces = (write_rows, read_rows, hist_write, hist_read)
         pieces = tuple(lax.all_gather(x, "tp", axis=2, tiled=True) for x in pieces)
         kv_rank = lax.axis_index("kv")
         bit_count = (group_span // lax.axis_size("tp")).bit_length() - 1
@@ -575,18 +592,24 @@
                 )
                 for mine, theirs in zip(pieces, partner)
             )
-    write_rows, read_rows, hist_write, hist_read = pieces
+        write_rows, read_rows, hist_write, hist_read = pieces
+        small = jnp.concatenate(
+            [
+                write_rows.astype(jnp.float32),
+                read_rows.astype(jnp.float32),
+                small[:, :, 2 * state_cols :],
+            ],
+            axis=2,
+        )
     unscaled, squares, base_state = mix(
         device_rank,
         device_rank // group_span,
         accepted[:, None],
-        steps,
         slab(last_steps),
         par,
         gate_rows,
         inner_rows,
-        write_rows,
-        read_rows,
+        small,
         hist_inner,
         hist_write,
         hist_read,

time: 81.1 us -> 70.8 us (0.87)
  Pallas kernels: 62.4 us -> 54.4 us
  matrix products: 9.22 us -> 5.32 us
  local copies, waits for them, and re-layouts: 4.37 us -> 6.02 us
    pallas_call x1, Pallas kernels: 23.9 us -> 15.9 us  [scattered(): pl.pallas_call(functools.partial(scatter_kernel, n), out_shape=[jax.Shape...]
    dot_general x5 -> x3, matrix products: 8.51 us -> 4.6 us  [project(): out = jnp.dot(normed, weight, preferred_element_type=jnp.float32)]
    unnamed x25 -> x24, local copies, waits for them, and re-layouts: 1.66 us -> 2.66 us
where the time goes in v3:
time: 70.8 us; the launch traced here: 70.3 us
  Pallas kernels  54.4 us (77%)
  local copies, waits for them, and re-layouts  6.02 us (9%)
  matrix products  5.32 us (8%)
  other arithmetic  3.76 us (5%)
  between operations  0.79 us (1%)
    pallas_call x1, Pallas kernels, mix(): pl.pallas_call(mix_kernel, grid_spec=pltpu.PrefetchScalarGridSpec(num_sca...  22.1 us
    pallas_call x1, Pallas kernels, gathered(): pl.pallas_call(functools.partial(gather_kernel, n), out_shape=jax.ShapeDt...  16.3 us
    pallas_call x1, Pallas kernels, scattered(): pl.pallas_call(functools.partial(scatter_kernel, n), out_shape=[jax.Shape...  15.9 us
    dot_general x3, matrix products, project(): out = jnp.dot(normed, weight, preferred_element_type=jnp.float32)  4.6 us
    unnamed x24, local copies, waits for them, and re-layouts  2.66 us

profile of v3, /device:TPU:0, one launch (start us, length us, event | category | flops | bytes accessed | tf_op | source)
XLA Modules:
  0.0 70.3 jit_solution(4608328074448717437)
XLA Ops:
  0.7 0.1 pad_add_fusion.rank_ref
  0.7 1.2 %fusion.26 = f32[32]{0:T(128)S(1)} fusion(bf16[32,2048]{1,0:T(8,128)(2,1)} %param.21), kind=kLoop, calls=%fused_computation.25 | loop fusion | flops 196576 | bytes 131200 | tf_op jit(solution)/shard_map/reduce_sum | solution.py:552
  1.9 0.7 %pad_maximum_fusion = f32[3,64]{1,0:T(4,128)S(1)} fusion(f32[1,64]{1,0:T(1,128)} %bitcast.51, f32[1,64]{1,0:T(1,128)} %bitcast.52, f32[1,64]{1,0:T(1,128)} %bitcast.53), kind=kLoop, calls=%fused_computation.39 | loop fusion | flops 384 | bytes 1536 | tf_op jit(solution)/shard_map/stack | solution.py:572
  2.6 0.1 constant_dynamic-slice_fusion.par_ref
  2.7 0.8 %constant_dynamic-slice_fusion.1 = bf16[2048,8]{0,1:T(8,128)(2,1)S(1)} fusion(bf16[2048,64]{0,1:T(8,128)(2,1)} %param.27, s32[]{:T(128)S(6)} %select_n.17), kind=kLoop, calls=%fused_computation.44 | loop fusion | bytes 65540 | tf_op jit(solution)/shard_map/dynamic_slice | solution.py:568
  3.5 0.7 %copy.31.acc_ref = s32[64,1]{1,0:T(8,128)S(1)} copy(s32[64,1]{0,1:T(1,128)} %bitcast.50) | data formatting | bytes 512 | tf_op jit(solution)/shard_map/broadcast_in_dim | solution.py:607
  4.2 1.0 %fusion.28.own_ref = bf16[32,2048]{1,0:T(8,128)(2,1)S(1)} fusion(bf16[32,2048]{1,0:T(8,128)(2,1)} %param.21, f32[2048]{0:T(1024)} %param.22, f32[32]{0:T(128)S(1)} %add_rsqrt_fusion.1), kind=kLoop, calls=%fused_computation.27 | loop fusion | flops 262144 | bytes 270464 | tf_op jit(solution)/shard_map/convert_element_type | solution.py:554
  5.2 0.8 %copy.30 = f32[64,4,8]{2,0,1:T(8,128)S(1)} copy(f32[64,4,8]{0,2,1:T(8,128)} %param.40) | data formatting | bytes 16384 | tf_op args[19]
  6.0 1.0 %copy.35 = bf16[2048,8]{1,0:T(8,128)(2,1)} copy(bf16[2048,8]{0,1:T(8,128)(2,1)S(1)} %constant_dynamic-slice_fusion.1) | data formatting | bytes 65536
  7.0 16.3 %gather.1 = bf16[4,2,32,2048]{3,2,1,0:T(8,128)(2,1)S(1)} custom-call(bf16[32,2048]{1,0:T(8,128)(2,1)S(1)} %fusion.28.own_ref), custom_call_target="tpu_custom_call" | custom-call | tf_op jit(solution)/shard_map/gather/pallas_call | solution.py:351
  23.4 1.2 %reshape_reshape.6 = bf16[64,4,2048]{2,1,0:T(4,128)(2,1)} reshape(bf16[4,2,32,2048]{3,2,1,0:T(8,128)(2,1)S(1)} %gather.1) | data formatting | bytes 2097152 | tf_op jit(solution)/shard_map/reshape;reshape | solution.py:556
  24.6 2.8 %fusion.7.steps_ref.write_ref.read_ref = f32[4,64,384]{2,1,0:T(8,128)S(1)} fusion(bf16[2048,8]{1,0:T(8,128)(2,1)} %copy.35, bf16[2048,128]{1,0:T(8,128)(2,1)} %param.26, bf16[2048,128]{1,0:T(8,128)(2,1)} %param.25, bf16[64,4,2048]{2,1,0:T(4,128)(2,1)} %reshape_reshape.6), kind=kOutput, calls=%fused_computation.9 | convolution fusion | flops 408944640 | bytes 2523136 | tf_op jit(solution)/shard_map/dot_general | solution.py:560
  27.4 0.9 %fusion.16.inner_ref = bf16[4,64,512]{2,1,0:T(8,128)(2,1)S(1)} fusion(bf16[2048,512]{1,0:T(8,128)(2,1)S(1)} %copy-done.9, bf16[64,4,2048]{2,1,0:T(4,128)(2,1)S(1)} %copy-done.8), kind=kOutput, calls=%fused_computation.15 | convolution fusion | flops 537001984 | bytes 3407872 | tf_op jit(solution)/shard_map/dot_general | solution.py:560
  28.3 0.7 copy-done.10
  29.0 0.9 %fusion.13.gate_ref = bf16[4,64,512]{2,1,0:T(8,128)(2,1)S(1)} fusion(bf16[2048,512]{1,0:T(8,128)(2,1)S(1)} %copy-done.10, bf16[64,4,2048]{2,1,0:T(4,128)(2,1)S(1)} %copy-done.8), kind=kOutput, calls=%fused_computation.14 | convolution fusion | flops 537001984 | bytes 3407872 | tf_op jit(solution)/shard_map/dot_general | solution.py:560
  30.1 22.1 %mix.1 = (bf16[4,64,512]{2,1,0:T(8,128)(2,1)S(1)}, f32[4,64,128]{2,1,0:T(8,128)S(1)}, f32[64,512,128]{2,1,0:T(8,128)}) custom-call(s32[2]{0:T(128)S(1)} %pad_add_fusion.rank_ref, s32[64,1]{1,0:T(8,128)S(1)} %copy.31.acc_ref, f32[4,64,384]{2,1,0:T(8,128)S(1)} %fusion.7.steps_ref.write_ref.read_ref, f32[4,64,8]{2,1,0:T(8,128)S(1)} %bitcast.41, ...), custom_call_target="tpu_custom_call" | custom-call | tf_op jit(solution)/shard_map/mix/pallas_call | solution.py:186
  52.2 0.2 copy.32
  52.4 0.1 reshape.78
  52.5 0.1 slice_reduce_fusion
  52.6 0.1 copy.33
  52.7 0.1 reshape_reshape.7
  52.8 0.7 %convolution_convert_fusion = bf16[256,2048]{1,0:T(8,128)(2,1)S(1)} fusion(bf16[256,512]{1,0:T(8,128)(2,1)S(1)} %reshape.78, bf16[512,2048]{1,0:T(8,128)(2,1)S(1)} %copy-done), kind=kOutput, calls=%fused_computation.2 | convolution fusion | flops 537395200 | bytes 3407872 | tf_op jit(solution)/shard_map/dot_general | solution.py:624
  53.5 15.9 %scatter.1 = (f32[32,2048]{1,0:T(8,128)S(1)}, f32[8,8,128]{2,1,0:T(8,128)S(1)}) custom-call(bf16[4,2,32,2048]{3,2,1,0:T(8,128)(2,1)S(1)} %bitcast.40, f32[8,8,128]{2,1,0:T(8,128)S(1)} %pad.9.sq), custom_call_target="tpu_custom_call" | custom-call | tf_op jit(solution)/shard_map/scatter/pallas_call | solution.py:499
  69.5 0.7 %multiply_convert_fusion = bf16[32,2048]{1,0:T(8,128)(2,1)} fusion(f32[32,2048]{1,0:T(8,128)S(1)} %get-tuple-element.9, f32[32]{0:T(128)S(1)} %add_rsqrt_fusion), kind=kLoop, calls=%fused_computation.28 | loop fusion | flops 131072 | bytes 393344 | tf_op jit(solution)/shard_map/convert_element_type | solution.py:627
  (27 shorter events, 0.2 us)
Async XLA Ops:
  0.6 52.2 %copy-start = (bf16[512,2048]{1,0:T(8,128)(2,1)S(1)}, bf16[512,2048]{1,0:T(8,128)(2,1)}, u32[]{:S(2)}) copy-start(bf16[512,2048]{1,0:T(8,128)(2,1)} %param.35) | copy-start | bytes 6291460
  24.6 2.8 %copy-start.8 = (bf16[64,4,2048]{2,1,0:T(4,128)(2,1)S(1)}, bf16[64,4,2048]{2,1,0:T(4,128)(2,1)}, u32[]{:S(2)}) copy-start(bf16[64,4,2048]{2,1,0:T(4,128)(2,1)} %reshape_reshape.6) | copy-start | bytes 3145732
  24.6 2.8 %copy-start.9 = (bf16[2048,512]{1,0:T(8,128)(2,1)S(1)}, bf16[2048,512]{1,0:T(8,128)(2,1)}, u32[]{:S(2)}) copy-start(bf16[2048,512]{1,0:T(8,128)(2,1)} %param.24) | copy-start | bytes 6291460
  27.4 1.6 %copy-start.10 = (bf16[2048,512]{1,0:T(8,128)(2,1)S(1)}, bf16[2048,512]{1,0:T(8,128)(2,1)}, u32[]{:S(2)}) copy-start(bf16[2048,512]{1,0:T(8,128)(2,1)} %param.23) | copy-start | bytes 6291460
  29.0 1.0 %copy-start.1 = (bf16[64,7,512]{2,0,1:T(8,128)(2,1)S(1)}, bf16[64,7,512]{2,0,1:T(8,128)(2,1)}, u32[]{:S(2)}) copy-start(bf16[64,7,512]{2,0,1:T(8,128)(2,1)} %param.37) | copy-start | bytes 1376260
  29.0 1.0 %copy-start.2 = (bf16[64,7,128]{2,0,1:T(8,128)(2,1)S(1)}, bf16[64,7,128]{2,0,1:T(8,128)(2,1)}, u32[]{:S(2)}) copy-start(bf16[64,7,128]{2,0,1:T(8,128)(2,1)} %param.38) | copy-start | bytes 344068
  29.0 1.1 %copy-start.3 = (bf16[64,7,128]{2,0,1:T(8,128)(2,1)S(1)}, bf16[64,7,128]{2,0,1:T(8,128)(2,1)}, u32[]{:S(2)}) copy-start(bf16[64,7,128]{2,0,1:T(8,128)(2,1)} %param.39) | copy-start | bytes 344068
  29.0 1.1 %copy-start.4 = (bf16[4,4096]{1,0:T(4,128)(2,1)S(1)}, bf16[4,4096]{1,0:T(4,128)(2,1)}, u32[]{:S(2)}) copy-start(bf16[4,4096]{1,0:T(4,128)(2,1)} %taps_inner_ref.1) | copy-start | bytes 98308
  29.0 1.1 %copy-start.5 = (f32[4096]{0:T(1024)S(1)}, f32[4096]{0:T(1024)}, u32[]{:S(2)}) copy-start(f32[4096]{0:T(1024)} %param.34) | copy-start | bytes 49156
  29.0 1.1 %copy-start.6 = (bf16[4,1024]{1,0:T(4,128)(2,1)S(1)}, bf16[4,1024]{1,0:T(4,128)(2,1)}, u32[]{:S(2)}) copy-start(bf16[4,1024]{1,0:T(4,128)(2,1)} %taps_write_ref.1) | copy-start | bytes 24580
  29.0 1.1 %copy-start.7 = (bf16[4,1024]{1,0:T(4,128)(2,1)S(1)}, bf16[4,1024]{1,0:T(4,128)(2,1)}, u32[]{:S(2)}) copy-start(bf16[4,1024]{1,0:T(4,128)(2,1)} %taps_read_ref.1) | copy-start | bytes 24580

commit v4 on v3

--- a/solution.py
+++ b/solution.py
@@ -225,7 +225,7 @@
 
 
 MESH = pl.DeviceIdType.MESH
-CHUNKS = 2
+CHUNKS = 4
 
 
 def remote(src, dst, send, recv, where):

time: 70.8 us -> 71.5 us (level)
    pallas_call x1, Pallas kernels: 15.9 us -> 17.2 us  [scattered(): pl.pallas_call(functools.partial(scatter_kernel, n), out_shape=[jax.Shape...]
where the time goes in v4:
time: 71.5 us; the launch traced here: 70.9 us
  Pallas kernels  55 us (77%)
  local copies, waits for them, and re-layouts  6.02 us (8%)
  matrix products  5.31 us (7%)
  other arithmetic  3.76 us (5%)
  between operations  0.79 us (1%)
    pallas_call x1, Pallas kernels, mix(): pl.pallas_call(mix_kernel, grid_spec=pltpu.PrefetchScalarGridSpec(num_sca...  22.1 us
    pallas_call x1, Pallas kernels, scattered(): pl.pallas_call(functools.partial(scatter_kernel, n), out_shape=[jax.Shape...  17.2 us
    pallas_call x1, Pallas kernels, gathered(): pl.pallas_call(functools.partial(gather_kernel, n), out_shape=jax.ShapeDt...  15.7 us
    dot_general x3, matrix products, project(): out = jnp.dot(normed, weight, preferred_element_type=jnp.float32)  4.6 us
    unnamed x24, local copies, waits for them, and re-layouts  2.66 us

profile of v4, /device:TPU:0, one launch (start us, length us, event | category | flops | bytes accessed | tf_op | source)
XLA Modules:
  0.0 70.9 jit_solution(12286349547990082807)
XLA Ops:
  0.7 0.1 pad_add_fusion.rank_ref
  0.7 1.2 %fusion.26 = f32[32]{0:T(128)S(1)} fusion(bf16[32,2048]{1,0:T(8,128)(2,1)} %param.21), kind=kLoop, calls=%fused_computation.25 | loop fusion | flops 196576 | bytes 131200 | tf_op jit(solution)/shard_map/reduce_sum | solution.py:552
  1.9 0.7 pad_maximum_fusion
  2.6 0.1 constant_dynamic-slice_fusion.par_ref
  2.7 0.8 %constant_dynamic-slice_fusion.1 = bf16[2048,8]{0,1:T(8,128)(2,1)S(1)} fusion(bf16[2048,64]{0,1:T(8,128)(2,1)} %param.27, s32[]{:T(128)S(6)} %select_n.17), kind=kLoop, calls=%fused_computation.44 | loop fusion | bytes 65540 | tf_op jit(solution)/shard_map/dynamic_slice | solution.py:568
  3.5 0.7 %copy.31.acc_ref = s32[64,1]{1,0:T(8,128)S(1)} copy(s32[64,1]{0,1:T(1,128)} %bitcast.50) | data formatting | bytes 512 | tf_op jit(solution)/shard_map/broadcast_in_dim | solution.py:607
  4.2 1.0 %fusion.28.own_ref = bf16[32,2048]{1,0:T(8,128)(2,1)S(1)} fusion(bf16[32,2048]{1,0:T(8,128)(2,1)} %param.21, f32[2048]{0:T(1024)} %param.22, f32[32]{0:T(128)S(1)} %add_rsqrt_fusion.1), kind=kLoop, calls=%fused_computation.27 | loop fusion | flops 262144 | bytes 270464 | tf_op jit(solution)/shard_map/convert_element_type | solution.py:554
  5.2 0.8 %copy.30 = f32[64,4,8]{2,0,1:T(8,128)S(1)} copy(f32[64,4,8]{0,2,1:T(8,128)} %param.40) | data formatting | bytes 16384 | tf_op args[19]
  6.0 1.0 %copy.35 = bf16[2048,8]{1,0:T(8,128)(2,1)} copy(bf16[2048,8]{0,1:T(8,128)(2,1)S(1)} %constant_dynamic-slice_fusion.1) | data formatting | bytes 65536
  7.0 15.7 %gather.1 = bf16[4,2,32,2048]{3,2,1,0:T(8,128)(2,1)S(1)} custom-call(bf16[32,2048]{1,0:T(8,128)(2,1)S(1)} %fusion.28.own_ref), custom_call_target="tpu_custom_call" | custom-call | tf_op jit(solution)/shard_map/gather/pallas_call | solution.py:351
  22.8 1.2 %reshape_reshape.6 = bf16[64,4,2048]{2,1,0:T(4,128)(2,1)} reshape(bf16[4,2,32,2048]{3,2,1,0:T(8,128)(2,1)S(1)} %gather.1) | data formatting | bytes 2097152 | tf_op jit(solution)/shard_map/reshape;reshape | solution.py:556
  24.0 2.8 %fusion.7.steps_ref.write_ref.read_ref = f32[4,64,384]{2,1,0:T(8,128)S(1)} fusion(bf16[2048,8]{1,0:T(8,128)(2,1)} %copy.35, bf16[2048,128]{1,0:T(8,128)(2,1)} %param.26, bf16[2048,128]{1,0:T(8,128)(2,1)} %param.25, bf16[64,4,2048]{2,1,0:T(4,128)(2,1)} %reshape_reshape.6), kind=kOutput, calls=%fused_computation.9 | convolution fusion | flops 408944640 | bytes 2523136 | tf_op jit(solution)/shard_map/dot_general | solution.py:560
  26.8 0.9 %fusion.16.inner_ref = bf16[4,64,512]{2,1,0:T(8,128)(2,1)S(1)} fusion(bf16[2048,512]{1,0:T(8,128)(2,1)S(1)} %copy-done.9, bf16[64,4,2048]{2,1,0:T(4,128)(2,1)S(1)} %copy-done.8), kind=kOutput, calls=%fused_computation.15 | convolution fusion | flops 537001984 | bytes 3407872 | tf_op jit(solution)/shard_map/dot_general | solution.py:560
  27.7 0.7 copy-done.10
  28.4 0.9 %fusion.13.gate_ref = bf16[4,64,512]{2,1,0:T(8,128)(2,1)S(1)} fusion(bf16[2048,512]{1,0:T(8,128)(2,1)S(1)} %copy-done.10, bf16[64,4,2048]{2,1,0:T(4,128)(2,1)S(1)} %copy-done.8), kind=kOutput, calls=%fused_computation.14 | convolution fusion | flops 537001984 | bytes 3407872 | tf_op jit(solution)/shard_map/dot_general | solution.py:560
  29.5 22.1 %mix.1 = (bf16[4,64,512]{2,1,0:T(8,128)(2,1)S(1)}, f32[4,64,128]{2,1,0:T(8,128)S(1)}, f32[64,512,128]{2,1,0:T(8,128)}) custom-call(s32[2]{0:T(128)S(1)} %pad_add_fusion.rank_ref, s32[64,1]{1,0:T(8,128)S(1)} %copy.31.acc_ref, f32[4,64,384]{2,1,0:T(8,128)S(1)} %fusion.7.steps_ref.write_ref.read_ref, f32[4,64,8]{2,1,0:T(8,128)S(1)} %bitcast.41, ...), custom_call_target="tpu_custom_call" | custom-call | tf_op jit(solution)/shard_map/mix/pallas_call | solution.py:186
  51.6 0.2 copy.32
  51.8 0.1 reshape.78
  51.9 0.1 slice_reduce_fusion
  52.0 0.1 copy.33
  52.1 0.1 reshape_reshape.7
  52.2 0.7 %convolution_convert_fusion = bf16[256,2048]{1,0:T(8,128)(2,1)S(1)} fusion(bf16[256,512]{1,0:T(8,128)(2,1)S(1)} %reshape.78, bf16[512,2048]{1,0:T(8,128)(2,1)S(1)} %copy-done), kind=kOutput, calls=%fused_computation.2 | convolution fusion | flops 537395200 | bytes 3407872 | tf_op jit(solution)/shard_map/dot_general | solution.py:624
  52.9 17.2 %scatter.1 = (f32[32,2048]{1,0:T(8,128)S(1)}, f32[8,8,128]{2,1,0:T(8,128)S(1)}) custom-call(bf16[4,2,32,2048]{3,2,1,0:T(8,128)(2,1)S(1)} %bitcast.40, f32[8,8,128]{2,1,0:T(8,128)S(1)} %pad.9.sq), custom_call_target="tpu_custom_call" | custom-call | tf_op jit(solution)/shard_map/scatter/pallas_call | solution.py:499
  70.1 0.7 %multiply_convert_fusion = bf16[32,2048]{1,0:T(8,128)(2,1)} fusion(f32[32,2048]{1,0:T(8,128)S(1)} %get-tuple-element.9, f32[32]{0:T(128)S(1)} %add_rsqrt_fusion), kind=kLoop, calls=%fused_computation.28 | loop fusion | flops 131072 | bytes 393344 | tf_op jit(solution)/shard_map/convert_element_type | solution.py:627
  (27 shorter events, 0.2 us)
Async XLA Ops:
  0.6 51.6 %copy-start = (bf16[512,2048]{1,0:T(8,128)(2,1)S(1)}, bf16[512,2048]{1,0:T(8,128)(2,1)}, u32[]{:S(2)}) copy-start(bf16[512,2048]{1,0:T(8,128)(2,1)} %param.35) | copy-start | bytes 6291460
  24.0 2.8 %copy-start.8 = (bf16[64,4,2048]{2,1,0:T(4,128)(2,1)S(1)}, bf16[64,4,2048]{2,1,0:T(4,128)(2,1)}, u32[]{:S(2)}) copy-start(bf16[64,4,2048]{2,1,0:T(4,128)(2,1)} %reshape_reshape.6) | copy-start | bytes 3145732
  24.0 2.8 %copy-start.9 = (bf16[2048,512]{1,0:T(8,128)(2,1)S(1)}, bf16[2048,512]{1,0:T(8,128)(2,1)}, u32[]{:S(2)}) copy-start(bf16[2048,512]{1,0:T(8,128)(2,1)} %param.24) | copy-start | bytes 6291460
  26.8 1.6 %copy-start.10 = (bf16[2048,512]{1,0:T(8,128)(2,1)S(1)}, bf16[2048,512]{1,0:T(8,128)(2,1)}, u32[]{:S(2)}) copy-start(bf16[2048,512]{1,0:T(8,128)(2,1)} %param.23) | copy-start | bytes 6291460
  28.4 1.0 %copy-start.1 = (bf16[64,7,512]{2,0,1:T(8,128)(2,1)S(1)}, bf16[64,7,512]{2,0,1:T(8,128)(2,1)}, u32[]{:S(2)}) copy-start(bf16[64,7,512]{2,0,1:T(8,128)(2,1)} %param.37) | copy-start | bytes 1376260
  28.4 1.0 %copy-start.2 = (bf16[64,7,128]{2,0,1:T(8,128)(2,1)S(1)}, bf16[64,7,128]{2,0,1:T(8,128)(2,1)}, u32[]{:S(2)}) copy-start(bf16[64,7,128]{2,0,1:T(8,128)(2,1)} %param.38) | copy-start | bytes 344068
  28.4 1.1 %copy-start.3 = (bf16[64,7,128]{2,0,1:T(8,128)(2,1)S(1)}, bf16[64,7,128]{2,0,1:T(8,128)(2,1)}, u32[]{:S(2)}) copy-start(bf16[64,7,128]{2,0,1:T(8,128)(2,1)} %param.39) | copy-start | bytes 344068
  28.4 1.1 %copy-start.4 = (bf16[4,4096]{1,0:T(4,128)(2,1)S(1)}, bf16[4,4096]{1,0:T(4,128)(2,1)}, u32[]{:S(2)}) copy-start(bf16[4,4096]{1,0:T(4,128)(2,1)} %taps_inner_ref.1) | copy-start | bytes 98308
  28.4 1.1 %copy-start.5 = (f32[4096]{0:T(1024)S(1)}, f32[4096]{0:T(1024)}, u32[]{:S(2)}) copy-start(f32[4096]{0:T(1024)} %param.34) | copy-start | bytes 49156
  28.4 1.1 %copy-start.6 = (bf16[4,1024]{1,0:T(4,128)(2,1)S(1)}, bf16[4,1024]{1,0:T(4,128)(2,1)}, u32[]{:S(2)}) copy-start(bf16[4,1024]{1,0:T(4,128)(2,1)} %taps_write_ref.1) | copy-start | bytes 24580
  28.4 1.1 %copy-start.7 = (bf16[4,1024]{1,0:T(4,128)(2,1)S(1)}, bf16[4,1024]{1,0:T(4,128)(2,1)}, u32[]{:S(2)}) copy-start(bf16[4,1024]{1,0:T(4,128)(2,1)} %taps_read_ref.1) | copy-start | bytes 24580
